TPU v7x, 256 devices: a whole 4x4x8 slice. The times are simulated.
256 devices in a mesh: kv: 32 (over z, y), tp: 8 (over x, core).
Axes of the slice: x: 4, y: 4, z: 8, core: 2. Of those that a mesh axis runs over, the one named last changes fastest.
Arguments:
- piece_tokens: bfloat16 [3072, 4096], P('kv'), may hold values from -6 to 6
- step_tokens: bfloat16 [32, 4096], P('kv'), may hold values from -6 to 6
- in_gain: float32 [4096], replicated, may hold values from 0.1 to 1.9
- w_query: bfloat16 [4096, 8, 2, 128], P(None, 'tp'), may hold values from -0.09375 to 0.09375
- w_key: bfloat16 [4096, 8, 2, 128], P(None, 'tp'), may hold values from -0.15625 to 0.15625
- w_value: bfloat16 [4096, 8, 256], P(None, 'tp'), may hold values from -0.09375 to 0.09375
- w_out: bfloat16 [8, 256, 4096], P('tp'), may hold values from -0.125 to 0.125
- mix_ratio: float32 [8], P('tp'), may hold values from 0.3 to 0.8
- out_gain: float32 [256], replicated, may hold values from 0.1 to 1.9
- prompt_keys: bfloat16 [65536, 8, 2, 128], P('kv', 'tp'), may hold values from -630 to 630
- prompt_values: bfloat16 [65536, 8, 256], P('kv', 'tp'), may hold values from -6 to 6
- step_cache_keys: bfloat16 [32, 4096, 8, 2, 128], P(None, 'kv', 'tp'), may hold values from -630 to 630
- step_cache_values: bfloat16 [32, 4096, 8, 256], P(None, 'kv', 'tp'), may hold values from -6 to 6
- prompt_len: int32 [1], replicated, may hold values from 64512 to 65536
- step_lens: int32 [32], replicated, may hold values from 4032 to 4096
Outputs:
- piece_out: bfloat16 [3072, 4096], P('kv', 'tp')
- step_out: bfloat16 [32, 4096], P('kv', 'tp')
- piece_keys: bfloat16 [3072, 8, 2, 128], P('kv', 'tp')
- piece_values: bfloat16 [3072, 8, 256], P('kv', 'tp')
- step_keys: bfloat16 [32, 8, 2, 128], P('kv', 'tp')
- step_values: bfloat16 [32, 8, 256], P('kv', 'tp')
Inputs may be any that keep to these rules, and one draw needn't show every extreme that they name: `prompt_len`: the piece's tokens follow these cached positions. `step_lens`: each decoding token follows its sequence's cached positions.
All inputs are finite; a program needn't handle non-finite values.
Results may differ from a plain program's by a relative error of at most 0.015.
Values may be sent and summed in bfloat16 or wider, within the bound.
A program may use at most 128 MiB of HBM per device.

v0:
```python
import math

import jax
import jax.numpy as jnp
from jax import lax
from jax.sharding import PartitionSpec as P

EPS = 1e-06
OUT_SCALE = 0.8


def laid_out(blocks, dim):
    blocks = jnp.moveaxis(blocks, 0, dim)
    lengths = blocks.shape
    return blocks.reshape(*lengths[:dim], lengths[dim] * lengths[dim + 1], *lengths[dim + 2 :])


def gather_together(arrays, axis, dims):
    ravelled = jnp.concatenate([a.reshape(-1) for a in arrays])
    lines, at, outs = (lax.all_gather(ravelled, axis), 0, [])
    for a, dim in zip(arrays, dims):
        blocks = lines[:, at : at + a.size].reshape(-1, *a.shape)
        outs.append(laid_out(blocks, dim))
        at += a.size
    return tuple(outs)


def sent_together(arrays, axis, split_dim, concat_dim, along):
    ends, at = ([], 0)
    for a in arrays[:-1]:
        at += a.shape[along]
        ends.append(at)
    both = jnp.concatenate(arrays, axis=along)
    return tuple(
        jnp.split(
            lax.all_to_all(both, axis, split_axis=split_dim, concat_axis=concat_dim, tiled=True),
            ends,
            axis=along,
        )
    )


def split_up(shard, dim, count):
    before, after = (shard.shape[:dim], shard.shape[dim + 1 :])
    return jnp.moveaxis(shard.reshape(*before, count, -1, *after), dim, 0)


def summed_on_arrival(shard, axis, dim):
    count = lax.axis_size(axis)
    blocks = lax.all_to_all(split_up(shard, dim, count), axis, 0, 0, tiled=True)
    return jnp.sum(blocks.astype(jnp.float32), axis=0)


def norm_rows(tokens, in_gain):
    floats = tokens.astype(jnp.float32)
    inv_rms = lax.rsqrt(jnp.mean(floats * floats, axis=-1, keepdims=True) + EPS)
    return (floats * inv_rms * in_gain).astype(jnp.bfloat16)


def project(normed, weight):
    flat_weight = weight.reshape(weight.shape[0], -1)
    product = jnp.dot(normed, flat_weight, preferred_element_type=jnp.float32)
    return product.astype(jnp.bfloat16).reshape((normed.shape[0],) + weight.shape[1:])


def piece_block(block_q, block_start, all_k, all_v, cache_ok, fresh_place):
    row_count = block_q.shape[0]
    row_place = block_start + jnp.arange(row_count, dtype=jnp.int32)
    visible = jnp.concatenate(
        [
            jnp.broadcast_to(cache_ok[None, :], (row_count, cache_ok.shape[0])),
            fresh_place[None, :] <= row_place[:, None],
        ],
        axis=1,
    )
    scores = jnp.einsum("qhcd,khcd->hcqk", block_q, all_k, preferred_element_type=jnp.float32)
    scores = scores * block_q.shape[-1] ** (-0.5)
    scores = jnp.where(visible[None, None], scores, -jnp.inf)
    maxima = jnp.max(scores, axis=-1)
    weights = jnp.exp(scores - maxima[..., None])
    totals = jnp.sum(weights, axis=-1)
    summed = jnp.einsum(
        "hcqk,khv->qhcv", weights.astype(jnp.bfloat16), all_v, preferred_element_type=jnp.float32
    )
    return (
        summed.astype(jnp.bfloat16),
        jnp.transpose(maxima, (2, 0, 1)),
        jnp.transpose(totals, (2, 0, 1)),
    )


def combine_parts(part_values, maxima, totals):
    row_best = jnp.max(maxima, axis=0)
    rescale = jnp.exp(maxima - row_best[None])
    return (
        jnp.sum(totals * rescale, axis=0),
        jnp.sum(part_values.astype(jnp.float32) * rescale[..., None], axis=0),
    )


def finish(norm_sum, value_sum, mix_ratio, out_gain):
    attended = value_sum / norm_sum[..., None]
    mixed = attended[:, :, 0] - mix_ratio[None, :, None] * attended[:, :, 1]
    inv_rms = lax.rsqrt(jnp.mean(mixed * mixed, axis=-1, keepdims=True) + EPS)
    return (mixed * inv_rms * out_gain[None, None, :] * OUT_SCALE).astype(jnp.bfloat16)


def on_device(
    piece_tokens,
    step_tokens,
    in_gain,
    w_query,
    w_key,
    w_value,
    w_out,
    mix_ratio,
    out_gain,
    prompt_keys,
    prompt_values,
    step_cache_keys,
    step_cache_values,
    prompt_len,
    step_lens,
):
    kv_place = lax.axis_index("kv")
    piece_dev = piece_tokens.shape[0]
    step_dev = step_tokens.shape[0]
    cache_dev = prompt_keys.shape[0]
    seq_count = step_cache_keys.shape[0]
    seq_cache = step_cache_keys.shape[1]
    all_rows = jnp.concatenate([piece_tokens, step_tokens], axis=0)
    normed = norm_rows(all_rows, in_gain)
    queries = project(normed, w_query)
    key_rows = project(normed, w_key)
    value_rows = project(normed, w_value)
    piece_k = key_rows[:piece_dev]
    step_k = key_rows[piece_dev:]
    piece_v = value_rows[:piece_dev]
    step_v = value_rows[piece_dev:]
    piece_q, step_q = gather_together((queries[:piece_dev], queries[piece_dev:]), "kv", (0, 0))
    all_k = jnp.concatenate([prompt_keys, piece_k], axis=0)
    all_v = jnp.concatenate([prompt_values, piece_v], axis=0)
    cache_ok = kv_place * cache_dev + jnp.arange(cache_dev, dtype=jnp.int32) < prompt_len[0]
    fresh_place = kv_place * piece_dev + jnp.arange(piece_dev, dtype=jnp.int32)
    piece_total = piece_q.shape[0]
    block_rows = math.gcd(piece_total, 512)
    blocks = piece_q.reshape((piece_total // block_rows, block_rows) + piece_q.shape[1:])
    starts = jnp.arange(piece_total // block_rows, dtype=jnp.int32) * block_rows

    def one_block(operands):
        return piece_block(operands[0], operands[1], all_k, all_v, cache_ok, fresh_place)

    summed, maxima, totals = lax.map(one_block, (blocks, starts))
    piece_sum = lax.optimization_barrier(summed.reshape((piece_total,) + summed.shape[2:]))
    piece_max = maxima.reshape((piece_total,) + maxima.shape[2:])
    piece_tot = totals.reshape((piece_total,) + totals.shape[2:])
    own_seq = jnp.arange(seq_count, dtype=jnp.int32) // step_dev == kv_place
    own_k = lax.dynamic_update_slice_in_dim(
        jnp.zeros((seq_count,) + step_k.shape[1:], jnp.bfloat16), step_k, kv_place * step_dev, 0
    )
    own_v = lax.dynamic_update_slice_in_dim(
        jnp.zeros((seq_count,) + step_v.shape[1:], jnp.bfloat16), step_v, kv_place * step_dev, 0
    )
    head_scale = step_q.shape[-1] ** (-0.5)
    cache_scores = (
        jnp.einsum("bhcd,bkhcd->bhck", step_q, step_cache_keys, preferred_element_type=jnp.float32)
        * head_scale
    )
    fresh_scores = (
        jnp.einsum("bhcd,bhcd->bhc", step_q, own_k, preferred_element_type=jnp.float32) * head_scale
    )
    cache_place = kv_place * seq_cache + jnp.arange(seq_cache, dtype=jnp.int32)
    cache_visible = cache_place[None, :] < step_lens[:, None]
    cache_scores = jnp.where(cache_visible[:, None, None, :], cache_scores, -jnp.inf)
    fresh_scores = jnp.where(own_seq[:, None, None], fresh_scores, -jnp.inf)
    step_max = jnp.maximum(jnp.max(cache_scores, axis=-1), fresh_scores)
    cache_weights = jnp.exp(cache_scores - step_max[..., None])
    fresh_weights = jnp.exp(fresh_scores - step_max)
    step_tot = jnp.sum(cache_weights, axis=-1) + fresh_weights
    fresh_rounded = lax.optimization_barrier(fresh_weights.astype(jnp.bfloat16))
    step_acc = jnp.einsum(
        "bhck,bkhv->bhcv",
        cache_weights.astype(jnp.bfloat16),
        step_cache_values,
        preferred_element_type=jnp.float32,
    )
    step_acc = (
        step_acc
        + fresh_rounded.astype(jnp.float32)[..., None] * own_v.astype(jnp.float32)[:, :, None, :]
    )
    step_sum = lax.optimization_barrier(step_acc.astype(jnp.bfloat16))
    value_parts = (
        lax.all_to_all(piece_sum[None], "kv", split_axis=1, concat_axis=0, tiled=True),
        lax.all_to_all(step_sum[None], "kv", split_axis=1, concat_axis=0, tiled=True),
    )
    stat_parts = (
        *sent_together((piece_max[None], piece_tot[None]), "kv", 1, 0, 2),
        *sent_together((step_max[None], step_tot[None]), "kv", 1, 0, 2),
    )
    piece_norm, piece_value = combine_parts(value_parts[0], stat_parts[0], stat_parts[1])
    step_norm, step_value = combine_parts(value_parts[1], stat_parts[2], stat_parts[3])
    headout = jnp.concatenate(
        [
            finish(piece_norm, piece_value, mix_ratio, out_gain),
            finish(step_norm, step_value, mix_ratio, out_gain),
        ],
        axis=0,
    )
    flat_heads = headout.reshape(headout.shape[0], -1)
    head_term = jnp.dot(
        flat_heads, w_out.reshape(-1, w_out.shape[-1]), preferred_element_type=jnp.float32
    ).astype(jnp.bfloat16)
    mixed = summed_on_arrival(head_term, "tp", 1).astype(jnp.bfloat16)
    return (mixed[:piece_dev], mixed[piece_dev:], piece_k, piece_v, step_k, step_v)


def solution(mesh):
    in_specs = (
        P("kv", None),
        P("kv", None),
        P(),
        P(None, "tp", None, None),
        P(None, "tp", None, None),
        P(None, "tp", None),
        P("tp", None, None),
        P("tp"),
        P(),
        P("kv", "tp", None, None),
        P("kv", "tp", None),
        P(None, "kv", "tp", None, None),
        P(None, "kv", "tp", None),
        P(),
        P(),
    )
    out_specs = (
        P("kv", "tp"),
        P("kv", "tp"),
        P("kv", "tp", None, None),
        P("kv", "tp", None),
        P("kv", "tp", None, None),
        P("kv", "tp", None),
    )
    return jax.shard_map(
        on_device, mesh=mesh, in_specs=in_specs, out_specs=out_specs, check_vma=False
    )
```

profile of v0, /device:TPU:1, one launch (start us, length us, event | category | flops | bytes accessed | tf_op | source)
XLA Modules:
  0.0 335.1 jit_solution(14767176631124233481)
XLA Ops:
  7.2 1.6 fusion.38
  8.8 2.5 fusion.44
  12.3 2.1 fusion.41
  15.0 2.2 fusion.47
  17.3 1.4 copy.76
  21.1 70.7 %all-gather.4.cloned.1.call-done = bf16[32,1,24832]{2,1,0:T(2,128)(2,1)} async-done(((bf16[1,1,24832]{2,1,0:T(2,128)(2,1)}), bf16[32,1,24832]{2,1,0:T(2,128)(2,1)}) %all-gather.4.cloned.1.call-update) | async-done | bytes 1589264 | tf_op jit(solution)/shard_map/all_gather | solution.py:20
  91.9 3.2 copy.139
  95.8 2.7 slice.76
  101.3 5.9 %all-to-all-start.3 = ((f32[1,32,2,2]{3,2,0,1:T(2,128)}), f32[1,32,2,2]{3,2,0,1:T(2,128)S(1)}, u32[]{:S(2)}, u32[]{:S(2)}) async-start(f32[1,32,2,2]{3,2,0,1:T(2,128)} %copy.91), calls=%async_computation.3 | async-start | bytes 65536 | tf_op jit(solution)/shard_map/all_to_all | solution.py:36
  107.2 2.3 reshape_reshape_reshape.3
  109.5 71.5 %while.15 = (s32[]{:T(128)}, bf16[6,512,1,2,256]{4,1,0,3,2:T(8,128)(2,1)}, f32[6,512,1,2]{1,3,2,0:T(2,128)S(1)}, f32[6,512,1,2]{1,3,2,0:T(2,128)S(1)}, s32[6]{0:...) while((s32[]{:T(128)}, ...), condition=%wide.region_4.5_spmd.clone, body=%wide.region_1.4_spmd.clone.sunk | while | flops 1711671936 | bytes 38777992 | solution.py:153
  111.5 2.1 pad_add_fusion.2
  113.8 1.8 fusion.90
  115.6 3.8 %fusion.91 = bf16[6,512,1,2,256]{4,1,0,3,2:T(8,128)(2,1)} fusion(bf16[6,512,1,2,256]{4,1,0,3,2:T(8,128)(2,1)} %get-tuple-element.293, s32[]{:T(128)S(6)} %copy.152, f32[2,512,2144]{1,2,0:T(8,128)S(1)} %get-tuple-element.275, f32[2,512]{1,0:T(2,128)S(1)} %get-tuple-element.276, pred[512,2144]{0,1:T(8,128)(4,1)S(1)} %pad_add_fusion.2, ...), kind=kOutput, calls=%fused_computation.12.clone.1 | convolution fusion | flops 1133117440 | bytes 11505668 | tf_op jit(solution)/shard_map/while/body/eval_jaxpr/hcqk,khv->qhcv/dot_general | solution.py:82
  119.4 2.0 fusion.92
  123.4 2.1 pad_add_fusion.2
  125.7 1.8 fusion.90
  127.5 3.8 %fusion.91 = bf16[6,512,1,2,256]{4,1,0,3,2:T(8,128)(2,1)} fusion(bf16[6,512,1,2,256]{4,1,0,3,2:T(8,128)(2,1)} %get-tuple-element.293, s32[]{:T(128)S(6)} %copy.152, f32[2,512,2144]{1,2,0:T(8,128)S(1)} %get-tuple-element.275, f32[2,512]{1,0:T(2,128)S(1)} %get-tuple-element.276, pred[512,2144]{0,1:T(8,128)(4,1)S(1)} %pad_add_fusion.2, ...), kind=kOutput, calls=%fused_computation.12.clone.1 | convolution fusion | flops 1133117440 | bytes 11505668 | tf_op jit(solution)/shard_map/while/body/eval_jaxpr/hcqk,khv->qhcv/dot_general | solution.py:82
  131.3 2.0 fusion.92
  135.3 2.1 pad_add_fusion.2
  137.6 1.8 fusion.90
  139.4 3.8 %fusion.91 = bf16[6,512,1,2,256]{4,1,0,3,2:T(8,128)(2,1)} fusion(bf16[6,512,1,2,256]{4,1,0,3,2:T(8,128)(2,1)} %get-tuple-element.293, s32[]{:T(128)S(6)} %copy.152, f32[2,512,2144]{1,2,0:T(8,128)S(1)} %get-tuple-element.275, f32[2,512]{1,0:T(2,128)S(1)} %get-tuple-element.276, pred[512,2144]{0,1:T(8,128)(4,1)S(1)} %pad_add_fusion.2, ...), kind=kOutput, calls=%fused_computation.12.clone.1 | convolution fusion | flops 1133117440 | bytes 11505668 | tf_op jit(solution)/shard_map/while/body/eval_jaxpr/hcqk,khv->qhcv/dot_general | solution.py:82
  143.2 2.0 fusion.92
  147.2 2.1 pad_add_fusion.2
  149.5 1.8 fusion.90
  151.3 3.8 %fusion.91 = bf16[6,512,1,2,256]{4,1,0,3,2:T(8,128)(2,1)} fusion(bf16[6,512,1,2,256]{4,1,0,3,2:T(8,128)(2,1)} %get-tuple-element.293, s32[]{:T(128)S(6)} %copy.152, f32[2,512,2144]{1,2,0:T(8,128)S(1)} %get-tuple-element.275, f32[2,512]{1,0:T(2,128)S(1)} %get-tuple-element.276, pred[512,2144]{0,1:T(8,128)(4,1)S(1)} %pad_add_fusion.2, ...), kind=kOutput, calls=%fused_computation.12.clone.1 | convolution fusion | flops 1133117440 | bytes 11505668 | tf_op jit(solution)/shard_map/while/body/eval_jaxpr/hcqk,khv->qhcv/dot_general | solution.py:82
  155.1 2.0 fusion.92
  159.2 2.1 pad_add_fusion.2
  161.4 1.8 fusion.90
  163.3 3.8 %fusion.91 = bf16[6,512,1,2,256]{4,1,0,3,2:T(8,128)(2,1)} fusion(bf16[6,512,1,2,256]{4,1,0,3,2:T(8,128)(2,1)} %get-tuple-element.293, s32[]{:T(128)S(6)} %copy.152, f32[2,512,2144]{1,2,0:T(8,128)S(1)} %get-tuple-element.275, f32[2,512]{1,0:T(2,128)S(1)} %get-tuple-element.276, pred[512,2144]{0,1:T(8,128)(4,1)S(1)} %pad_add_fusion.2, ...), kind=kOutput, calls=%fused_computation.12.clone.1 | convolution fusion | flops 1133117440 | bytes 11505668 | tf_op jit(solution)/shard_map/while/body/eval_jaxpr/hcqk,khv->qhcv/dot_general | solution.py:82
  167.0 2.0 fusion.92
  171.1 2.1 pad_add_fusion.2
  173.3 1.8 fusion.90
  175.2 3.8 %fusion.91 = bf16[6,512,1,2,256]{4,1,0,3,2:T(8,128)(2,1)} fusion(bf16[6,512,1,2,256]{4,1,0,3,2:T(8,128)(2,1)} %get-tuple-element.293, s32[]{:T(128)S(6)} %copy.152, f32[2,512,2144]{1,2,0:T(8,128)S(1)} %get-tuple-element.275, f32[2,512]{1,0:T(2,128)S(1)} %get-tuple-element.276, pred[512,2144]{0,1:T(8,128)(4,1)S(1)} %pad_add_fusion.2, ...), kind=kOutput, calls=%fused_computation.12.clone.1 | convolution fusion | flops 1133117440 | bytes 11505668 | tf_op jit(solution)/shard_map/while/body/eval_jaxpr/hcqk,khv->qhcv/dot_general | solution.py:82
  178.9 2.0 fusion.92
  181.0 2.6 fusion.56
  183.7 9.4 %all-to-all-start.2 = ((bf16[1,32,1,2,256]{4,3,2,0,1:T(2,128)(2,1)}), bf16[1,32,1,2,256]{4,3,2,0,1:T(2,128)(2,1)S(1)}, u32[]{:S(2)}, u32[]{:S(2)}) async-start(bf16[1,32,1,2,256]{4,3,2,0,1:T(2,128)(2,1)} %bitcast.21), calls=%async_computation.2 | async-start | bytes 65536 | tf_op jit(solution)/shard_map/all_to_all | solution.py:194
  193.1 2.9 copy.82
  196.0 5.2 %reshape.499 = f32[32,1,384]{2,1,0:T(1,128)} reshape(f32[3072,1,2,2]{3,2,1,0:T(2,128)S(1)} %bitcast.157) | data formatting | bytes 98304
  201.8 8.6 %all-to-all-start.1 = ((f32[32,1,384]{2,1,0:T(1,128)}), f32[32,1,384]{2,1,0:T(1,128)S(1)}, u32[]{:S(2)}, u32[]{:S(2)}) async-start(f32[32,1,384]{2,1,0:T(1,128)} %reshape.499), calls=%async_computation.1 | async-start | bytes 98304 | tf_op jit(solution)/shard_map/all_to_all | solution.py:36
  210.4 8.0 %copy.80 = bf16[1,3072,1,2,256]{4,3,2,0,1:T(2,128)(2,1)} copy(bf16[1,3072,1,2,256]{4,1,3,2,0:T(8,128)(2,1)} %bitcast.161) | data formatting | bytes 6291456 | tf_op jit(solution)/shard_map/broadcast_in_dim | solution.py:193
  219.1 8.7 %all-to-all-start = ((bf16[1,3072,1,2,256]{4,3,2,0,1:T(2,128)(2,1)}), bf16[1,3072,1,2,256]{4,3,2,0,1:T(2,128)(2,1)}, u32[]{:S(2)}, u32[]{:S(2)}) async-start(bf16[1,3072,1,2,256]{4,3,2,0,1:T(2,128)(2,1)} %copy.80), calls=%async_computation | async-start | bytes 6291456 | tf_op jit(solution)/shard_map/all_to_all | solution.py:193
  231.8 4.8 %reshape.500 = f32[3072,1,2,2]{3,2,1,0:T(2,128)S(1)} reshape(f32[32,384]{1,0:T(8,128)S(1)} %reduce.25) | data formatting | bytes 98304
  236.6 4.9 %fusion.81 = (f32[32,96,1,2]{3,2,1,0:T(1,128)}, f32[96,2]{1,0:T(8,128)S(1)}, f32[32,96,1,2]{3,2,1,0:T(1,128)}) fusion(f32[32,96,2,2]{3,2,1,0:T(2,128)S(1)} %bitcast.156), kind=kLoop, calls=%fused_computation.114 | loop fusion | flops 5952 | bytes 99072 | tf_op jit(solution)/shard_map/split | solution.py:35
  241.5 2.6 copy.109
  245.1 48.3 %all-to-all-done = bf16[1,3072,1,2,256]{4,3,2,0,1:T(2,128)(2,1)} async-done(((bf16[1,3072,1,2,256]{4,3,2,0,1:T(2,128)(2,1)}), bf16[1,3072,1,2,256]{4,3,2,0,1:T(2,128)(2,1)}, u32[]{:S(2)}, u32[]{:S(2)}) %all-to-all-start) | async-done | bytes 3145760 | tf_op jit(solution)/shard_map/all_to_all | solution.py:193
  293.4 4.5 %convert.8 = f32[32,96,1,2,256]{4,3,1,0,2:T(2,128)S(1)} convert(bf16[32,96,1,2,256]{4,3,1,0,2:T(2,128)(2,1)} %bitcast.49) | non-fusion elementwise | flops 1572864 | bytes 9437184 | tf_op jit(solution)/shard_map/convert_element_type | solution.py:97
  300.6 26.3 %all_to_all.47 = bf16[8,97,512]{2,1,0:T(8,128)(2,1)S(1)} all-to-all(bf16[8,97,512]{2,1,0:T(8,128)(2,1)S(1)} %bitcast.158), channel_id=1, replica_groups=mesh['kv'=32,'tp'=8] {'tp'}, dimensions={0} | all-to-all | bytes 1589248 | tf_op jit(solution)/shard_map/all_to_all | solution.py:50
  (164 shorter events, 29.0 us)
Async XLA Ops:
  7.2 91.5 %copy-start = (bf16[32,128,1,2,128]{4,3,2,1,0:T(2,128)(2,1)S(1)}, bf16[32,128,1,2,128]{4,3,2,1,0:T(2,128)(2,1)}, u32[]{:S(2)}) copy-start(bf16[32,128,1,2,128]{4,3,2,1,0:T(2,128)(2,1)} %param.28) | copy-start | bytes 6291460
  7.2 84.7 %all-gather.4.cloned.1.call-start = ((), (), s32[]{:S(2)}) async-start(), calls=%async_computation.5 | async-start | bytes 3277824 | tf_op jit(solution)/shard_map/all_gather | solution.py:20
  8.8 3.4 %copy-start.7 = (bf16[96,4096]{1,0:T(8,128)(2,1)S(1)}, bf16[96,4096]{1,0:T(8,128)(2,1)}, u32[]{:S(2)}) copy-start(bf16[96,4096]{1,0:T(8,128)(2,1)} %param.17) | copy-start | bytes 2359300
  8.8 3.4 %copy-start.10 = (bf16[1,4096]{1,0:T(2,128)(2,1)S(1)}, bf16[1,4096]{1,0:T(2,128)(2,1)}, u32[]{:S(2)}) copy-start(bf16[1,4096]{1,0:T(2,128)(2,1)} %param.18) | copy-start | bytes 24580
  8.8 3.4 %copy-start.13 = (f32[4096]{0:T(1024)S(1)}, f32[4096]{0:T(1024)}, u32[]{:S(2)}) copy-start(f32[4096]{0:T(1024)} %param.19) | copy-start | bytes 49156
  17.2 1.6 copy-start.12
  17.2 2.7 copy-start.8
  18.6 1.3 copy-start.6
  18.7 2.4 copy-start.14
  18.8 2.3 copy-start.9
  99.9 9.7 %copy-start.4 = (bf16[2144,1,2,128]{3,0,2,1:T(8,128)(2,1)S(1)}, bf16[2144,1,2,128]{3,0,2,1:T(8,128)(2,1)}, u32[]{:S(2)}) copy-start(bf16[2144,1,2,128]{3,0,2,1:T(8,128)(2,1)} %pad_maximum_fusion) | copy-start | bytes 3293188
  101.3 82.4 %all-to-all-start.3 = ((f32[1,32,2,2]{3,2,0,1:T(2,128)}), f32[1,32,2,2]{3,2,0,1:T(2,128)S(1)}, u32[]{:S(2)}, u32[]{:S(2)}) async-start(f32[1,32,2,2]{3,2,0,1:T(2,128)} %copy.91), calls=%async_computation.3 | async-start | bytes 65536 | tf_op jit(solution)/shard_map/all_to_all | solution.py:36
  113.7 1.8 copy-start.5
  125.7 1.8 copy-start.5
  137.6 1.8 copy-start.5
  149.5 1.9 copy-start.5
  161.4 1.8 copy-start.5
  173.3 1.9 copy-start.5
  183.7 18.1 %all-to-all-start.2 = ((bf16[1,32,1,2,256]{4,3,2,0,1:T(2,128)(2,1)}), bf16[1,32,1,2,256]{4,3,2,0,1:T(2,128)(2,1)S(1)}, u32[]{:S(2)}, u32[]{:S(2)}) async-start(bf16[1,32,1,2,256]{4,3,2,0,1:T(2,128)(2,1)} %bitcast.21), calls=%async_computation.2 | async-start | bytes 65536 | tf_op jit(solution)/shard_map/all_to_all | solution.py:194
  201.8 17.4 %all-to-all-start.1 = ((f32[32,1,384]{2,1,0:T(1,128)}), f32[32,1,384]{2,1,0:T(1,128)S(1)}, u32[]{:S(2)}, u32[]{:S(2)}) async-start(f32[32,1,384]{2,1,0:T(1,128)} %reshape.499), calls=%async_computation.1 | async-start | bytes 98304 | tf_op jit(solution)/shard_map/all_to_all | solution.py:36
  218.3 12.1 %copy-start.11 = (f32[256]{0:T(256)S(1)}, f32[256]{0:T(256)}, u32[]{:S(2)}) copy-start(f32[256]{0:T(256)} %param.25) | copy-start | bytes 3076
  219.1 74.2 %all-to-all-start = ((bf16[1,3072,1,2,256]{4,3,2,0,1:T(2,128)(2,1)}), bf16[1,3072,1,2,256]{4,3,2,0,1:T(2,128)(2,1)}, u32[]{:S(2)}, u32[]{:S(2)}) async-start(bf16[1,3072,1,2,256]{4,3,2,0,1:T(2,128)(2,1)} %copy.80), calls=%async_computation | async-start | bytes 6291456 | tf_op jit(solution)/shard_map/all_to_all | solution.py:193
  241.5 2.6 copy-start.2
  297.9 1.6 copy-start.3
  300.3 28.0 %copy-start.1 = (bf16[32,128,1,2,128]{4,3,2,1,0:T(2,128)(2,1)S(1)}, bf16[32,128,1,2,128]{4,3,2,1,0:T(2,128)(2,1)}, u32[]{:S(2)}) copy-start(bf16[32,128,1,2,128]{4,3,2,1,0:T(2,128)(2,1)} %param.28) | copy-start | bytes 6291460
Sparse Core Ops, SparseCore 0:
  12.3 79.5 all-gather.3
where the time goes:
time: 336 us; the launch traced here: 335 us
  waiting for transfers between devices  120 us (36%)
  other arithmetic  49.7 us (15%)
  local copies, waits for them, and re-layouts  44.8 us (13%)
  matrix products  44.8 us (13%)
  starting transfers between devices  32.7 us (10%)
  blocking collectives  26.3 us (8%)
  between operations  15.9 us (5%)
    all_gather x1, waiting for transfers between devices, gather_together(): lines, at, outs = (lax.all_gather(ravelled, axis), 0, [])  70.7 us
    all_to_all x1, waiting for transfers between devices, on_device(): lax.all_to_all(piece_sum[None], 'kv', split_axis=1, concat_axis=0, tiled=...  48.3 us
    all_to_all x1, blocking collectives, summed_on_arrival(): blocks = lax.all_to_all(split_up(shard, dim, count), axis, 0, 0, tiled=True)  26.3 us
    dot_general x6, matrix products, piece_block(): jnp.einsum('hcqk,khv->qhcv', weights.astype(jnp.bfloat16), all_v, preferr...  22.6 us
    unnamed x39, local copies, waits for them, and re-layouts  19.4 us
    all_to_all x2, starting transfers between devices, sent_together(): lax.all_to_all(both, axis, split_axis=split_dim, concat_axis=concat_dim,...  14.5 us
    concatenate x6, other arithmetic, piece_block(): jnp.concatenate([jnp.broadcast_to(cache_ok[None, :], (row_count, cache_ok...  12.3 us
    reduce_sum x6, other arithmetic, piece_block(): totals = jnp.sum(weights, axis=-1)  12.3 us
  transfers between devices with their start and end apart: 5, of which 4 were waited for; matrix products, arithmetic and copies ran while one was open for 35% of the time, Pallas kernels for 0%

commit v1 on v0

v1 whole, which is shorter than its diff:
```python
import functools
import math

import jax
import jax.numpy as jnp
from jax import lax
from jax.experimental import pallas as pl
from jax.experimental.pallas import tpu as pltpu
from jax.sharding import PartitionSpec as P

EPS = 1e-06
OUT_SCALE = 0.8
NZ, NY, NKV = 8, 4, 32
ROWS = 96
CHUNKS = 3
R = ROWS // CHUNKS
RD = 16
TILE = NZ * R
TILED = NZ * RD
CACHE = 2048
KEYS = CACHE + 128
SEQC = 128
DH, DV = 128, 256
PADDED = ROWS + RD
EXPC = DH ** (-0.5) * math.log2(math.e)
STAT_Z = (1, 3, 5, 7)
F32, BF16 = jnp.float32, jnp.bfloat16
NT = (((1,), (1,)), ((), ()))


def attend(
    q_own, k_own, v_own, kp_hbm, vp_hbm, kd_hbm, vd_hbm, gain_ref, plen, slens, mix,
    out_ref,
    kbuf, vnat, vt, kd, vdn, vtd, ksd, vse, qall, qd, bias, sbuf, pbuf, oacc, oaccd,
    stat, srecv, ressend, res, comb, combd, rh, rhd, rf, rfd, acc, accb, accbd, rz, rzd, mixed,
    load_sem, zs, zr, ys, yr, hs, hr, ss, sr, rs, rr, xs, xr, fs, fr, ws, wr,
):
    me = lax.axis_index("kv")
    z = me // NY
    y = me % NY
    yp, ym, y2 = (y + 1) % NY, (y + 3) % NY, (y + 2) % NY

    def at_kv(index):
        return {"kv": index}

    def rcopy(src, dst, s_sem, r_sem, target):
        return pltpu.make_async_remote_copy(
            src_ref=src, dst_ref=dst, send_sem=s_sem, recv_sem=r_sem,
            device_id=at_kv(target), device_id_type=pl.DeviceIdType.MESH,
        )

    def rows_of(j):
        return R if j < CHUNKS else RD

    def qtile(j, yy):
        return qall.at[j * NY + yy] if j < CHUNKS else qd.at[yy]

    def ctile(j, yy):
        return comb.at[j * NY + yy] if j < CHUNKS else combd.at[yy]

    def zblock(view, zz, n):
        return view.at[pl.ds(pl.multiple_of(zz * n, n), n), :]

    barrier = pltpu.get_barrier_semaphore()

    @pl.loop(1, NKV)
    def _(d):
        pl.semaphore_signal(
            barrier, inc=1, device_id=at_kv((me + d) % NKV),
            device_id_type=pl.DeviceIdType.MESH,
        )

    loads = [
        pltpu.make_async_copy(kp_hbm, kbuf.at[pl.ds(0, CACHE), :], load_sem.at[0]),
        pltpu.make_async_copy(vp_hbm, vnat, load_sem.at[1]),
        pltpu.make_async_copy(kd_hbm, kd, load_sem.at[2]),
        pltpu.make_async_copy(vd_hbm, vdn, load_sem.at[3]),
    ]
    for load in loads:
        load.start()

    for j in range(4):
        n = rows_of(j)
        lo = j * R if j < CHUNKS else ROWS
        mine = qtile(j, y)
        mine[pl.ds(pl.multiple_of(z * n, n), n), :] = q_own[lo : lo + n, :]

    pl.semaphore_wait(barrier, NKV - 1)

    def z_copy(j, d):
        n = rows_of(j)
        zt = (z + d) % NZ
        block = zblock(qtile(j, y), z, n)
        return rcopy(block, block, zs.at[j, d], zr.at[j, d], zt * NY + y)

    for j in range(4):
        for d in (1, 7, 2, 6, 3, 5, 4):
            z_copy(j, d).start()

    kbuf[CACHE : CACHE + ROWS, :] = k_own[:ROWS, :]
    kbuf[CACHE + ROWS :, :] = jnp.zeros((KEYS - CACHE - ROWS, 2 * DH), BF16)
    ksd[:RD, :] = k_own[ROWS:, :]
    ksd[RD:, :] = jnp.zeros((SEQC - RD, 2 * DH), BF16)
    tail = jnp.concatenate([v_own[:ROWS, :], jnp.zeros((128 - ROWS, DV), BF16)], axis=0)
    vt[:, CACHE:] = tail.T
    tail = jnp.concatenate([v_own[ROWS:, :], jnp.zeros((128 - RD, DV), BF16)], axis=0)
    vse[...] = tail.T
    half = CACHE // 2
    place = me * CACHE + half + lax.broadcasted_iota(jnp.int32, (half, 128), 0)
    bias[...] = jnp.where(place < plen[0], 0.0, -jnp.inf).astype(F32)
    loads[0].wait()
    loads[1].wait()
    for b in range(CACHE // 256):
        vt[:, b * 256 : (b + 1) * 256] = vnat[b * 256 : (b + 1) * 256, :].T

    def z_wait_y_send(j):
        n = rows_of(j)
        for d in range(1, NZ):
            zf = (z + NZ - d) % NZ
            block = zblock(qtile(j, y), zf, n)
            rcopy(block, block, zs.at[j, d], zr.at[j, d], zf * NY + y).wait_recv()
        y_copy(j, 0).start()
        y_copy(j, 1).start()

    def y_copy(j, side):
        tile = qtile(j, y)
        return rcopy(tile, tile, ys.at[j, side], yr.at[j, side], z * NY + (yp if side == 0 else ym))

    def half_of(view, j, side):
        h = NZ * rows_of(j) // 2
        return view.at[pl.ds(side * h, h), :]

    def h_copy(j, side):
        part = half_of(qtile(j, ym if side == 0 else yp), j, side)
        return rcopy(part, part, hs.at[j, side], hr.at[j, side], z * NY + (yp if side == 0 else ym))

    def y_wait_fwd(j):
        for side in (0, 1):
            tile = qtile(j, ym if side == 0 else yp)
            rcopy(tile, tile, ys.at[j, side], yr.at[j, side], z * NY + y2).wait_recv()
            h_copy(j, side).start()

    def h_wait(j):
        for side in (0, 1):
            part = half_of(qtile(j, y2), j, side)
            rcopy(part, part, hs.at[j, side], hr.at[j, side], z * NY + y2).wait_recv()

    KB = [(b * 256, 256) for b in range(CACHE // 256)] + [(CACHE, 128)]

    @pl.loop(0, CHUNKS * NY)
    def _(t):
        for step, work in (
            (0, lambda: z_wait_y_send(0)),
            (1, lambda: z_wait_y_send(1)),
            (1, lambda: y_wait_fwd(0)),
            (2, lambda: z_wait_y_send(2)),
            (3, lambda: h_wait(0)),
            (3, lambda: z_wait_y_send(3)),
            (4, lambda: y_wait_fwd(1)),
            (5, lambda: y_wait_fwd(2)),
            (6, lambda: y_wait_fwd(3)),
            (7, lambda: h_wait(1)),
            (11, lambda: h_wait(2)),
        ):
            pl.when(t == step)(work)

        j = t // NY
        i = t % NY
        yy = (y + jnp.where(i == 2, 3, jnp.where(i == 3, 2, i))) % NY
        tt = j * NY + yy
        lane = lax.broadcasted_iota(jnp.int32, (128, TILE), 1)
        row = lax.broadcasted_iota(jnp.int32, (128, TILE), 0)
        row_place = ((lane // R) * NY + yy) * ROWS + R * j + lane % R
        fresh_ok = (row < ROWS) & (me * ROWS + row <= row_place)
        for c in range(2):
            cols = slice(c * DH, (c + 1) * DH)
            q = qall[tt, :, cols]
            top = jnp.full((8, TILE), -jnp.inf, F32)
            for at, size in KB:
                s = lax.dot_general(kbuf[at : at + size, cols], q, NT, preferred_element_type=F32)
                if at == CACHE:
                    s = jnp.where(fresh_ok, s, -jnp.inf)
                elif at >= half:
                    b = bias[at - half : at - half + size, :]
                    s = s + jnp.concatenate([b, b], axis=1)
                sbuf[c, at : at + size, :] = s
                top = jnp.maximum(top, jnp.max(s.reshape(size // 8, 8, TILE), axis=0))
            m = jnp.max(top, axis=0, keepdims=True)
            total = jnp.zeros((8, TILE), F32)
            for at, size in KB:
                w = jnp.exp2((sbuf[c, at : at + size, :] - m) * EXPC)
                total = total + jnp.sum(w.reshape(size // 8, 8, TILE), axis=0)
                pbuf[c, at : at + size, :] = w.astype(BF16)
            total = jnp.sum(total, axis=0, keepdims=True)
            oacc[tt, c] = jnp.dot(vt[...], pbuf[c], preferred_element_type=F32)
            for hh in range(2):
                stat[tt, 2 * c + hh : 2 * c + hh + 1, :] = m[:, hh * 128 : (hh + 1) * 128]
                stat[tt, 4 + 2 * c + hh : 5 + 2 * c + hh, :] = total[:, hh * 128 : (hh + 1) * 128]

    loads[2].wait()
    loads[3].wait()
    h_wait(3)

    @pl.loop(0, NY)
    def _(yy):
        q2 = qd[yy]
        lane = lax.broadcasted_iota(jnp.int32, (SEQC, TILED), 1)
        row = lax.broadcasted_iota(jnp.int32, (SEQC, TILED), 0)
        own = (lane // RD == jnp.where(yy == y, z, NZ)) & (row == 0)
        for zz in range(NZ):
            vtd[:, zz * SEQC : (zz + 1) * SEQC] = vdn[zz * NY + yy].T
        stat[CHUNKS * NY + yy] = jnp.where(lax.broadcasted_iota(jnp.int32, (8, 128), 0) < 4, 0.0, 1.0)
        for c in range(2):
            cols = slice(c * DH, (c + 1) * DH)
            q = q2[:, cols]
            parts = []
            top = jnp.full((8, TILED), -jnp.inf, F32)
            for zz in range(NZ + 1):
                if zz < NZ:
                    k = kd[zz * NY + yy, :, cols]
                    ok = (lane // RD == zz) & (me * SEQC + row < slens[zz * NY + yy])
                else:
                    k = ksd[:, cols]
                    ok = own
                s = lax.dot_general(k, q, NT, preferred_element_type=F32)
                s = jnp.where(ok, s, -jnp.inf)
                parts.append(s)
                top = jnp.maximum(top, jnp.max(s.reshape(SEQC // 8, 8, TILED), axis=0))
            m = jnp.max(top, axis=0, keepdims=True)
            total = jnp.zeros((8, TILED), F32)
            out = jnp.zeros((DV, TILED), F32)
            for zz in range(NZ + 1):
                w = jnp.exp2((parts[zz] - m) * EXPC)
                total = total + jnp.sum(w.reshape(SEQC // 8, 8, TILED), axis=0)
                v = vtd[:, zz * SEQC : (zz + 1) * SEQC] if zz < NZ else vse[...]
                out = out + jnp.dot(v, w.astype(BF16), preferred_element_type=F32)
            oaccd[yy, c] = out
            stat[CHUNKS * NY + yy, 2 * c : 2 * c + 1, :] = m
            stat[CHUNKS * NY + yy, 4 + 2 * c : 5 + 2 * c, :] = jnp.sum(total, axis=0, keepdims=True)

    def s_copy(j, yt):
        return rcopy(
            stat.at[j * NY + yt], srecv.at[j, me], ss.at[j, yt], sr.at[j, me], STAT_Z[j] * NY + yt
        )

    def stats_send(j):
        for yt in range(NY):
            target = STAT_Z[j] * NY + yt

            @pl.when(target != me)
            def _():
                s_copy(j, yt).start()

            @pl.when(target == me)
            def _():
                srecv[j, me] = stat[j * NY + yt]

    def r_copy(j, target):
        return rcopy(ressend.at[j], res.at[j * NY + y], rs.at[j, target], rr.at[j, y], target)

    def stats_own(j):
        @pl.when(z == STAT_Z[j])
        def _():
            @pl.loop(1, NKV)
            def _(d):
                src = (me + d) % NKV
                rcopy(stat.at[0], srecv.at[j, src], ss.at[j, 0], sr.at[j, src], src).wait_recv()

            every = srecv[j]
            best = jnp.max(every[:, 0:4, :], axis=0)
            norm = jnp.sum(every[:, 4:8, :] * jnp.exp2((every[:, 0:4, :] - best[None]) * EXPC), axis=0)
            both = jnp.concatenate([best, 1.0 / norm], axis=0)
            ressend[j] = both
            res[j * NY + y] = both

            @pl.loop(1, NKV)
            def _(d):
                r_copy(j, (me + d) % NKV).start()

    def stats_wait(j):
        for yt in range(NY):
            owner = STAT_Z[j] * NY + yt

            @pl.when(owner != me)
            def _():
                rcopy(ressend.at[j], res.at[j * NY + yt], rs.at[j, owner], rr.at[j, yt], owner).wait_recv()

    for j in range(4):
        stats_send(j)
    for j in range(4):
        stats_own(j)

    def combine(j):
        wide = 2 if j < CHUNKS else 1

        @pl.loop(0, NY)
        def _(yy):
            tt = j * NY + yy
            factors = []
            for c in range(2):
                pick = lambda ref, lo: jnp.concatenate(
                    [ref[tt, lo + 2 * c + hh : lo + 2 * c + hh + 1, :] for hh in range(wide)], axis=1
                )
                factors.append(jnp.exp2((pick(stat, 0) - pick(res, 0)) * EXPC) * pick(res, 4))
            values = oacc if j < CHUNKS else oaccd
            at = tt if j < CHUNKS else yy
            both = values[at, 0] * factors[0] - values[at, 1] * (factors[1] * mix[0])
            ctile(j, yy)[...] = both.T.astype(BF16)

    def x_copy(j, side):
        part = half_of(ctile(j, y2), j, side)
        land = rh.at[j, side] if j < CHUNKS else rhd.at[side]
        return rcopy(part, land, xs.at[j, side], xr.at[j, side], z * NY + (yp if side == 0 else ym))

    def f_copy(j, side):
        tile = ctile(j, yp if side == 0 else ym)
        land = rf.at[j, side] if j < CHUNKS else rfd.at[side]
        return rcopy(tile, land, fs.at[j, side], fr.at[j, side], z * NY + (yp if side == 0 else ym))

    def rs_second(j):
        h = NZ * rows_of(j) // 2
        for side in (0, 1):
            x_copy(j, side).wait_recv()
            land = rh[j, side] if j < CHUNKS else rhd[side]
            part = half_of(ctile(j, yp if side == 0 else ym), j, side)
            part[...] = (part[...].astype(F32) + land.astype(F32)).astype(BF16)
            f_copy(j, side).start()

    def wire_block(j, zz):
        n = rows_of(j)
        return zblock(accb.at[j] if j < CHUNKS else accbd, zz, n)

    def w_copy(j, d):
        zt = (z + d) % NZ
        land = rz.at[j, d] if j < CHUNKS else rzd.at[d]
        return rcopy(wire_block(j, zt), land, ws.at[j, d], wr.at[j, d], zt * NY + y)

    def rs_third(j):
        n = rows_of(j)
        for side in (0, 1):
            f_copy(j, side).wait_recv()
        if j < CHUNKS:
            total = comb[j * NY + y].astype(F32) + rf[j, 0].astype(F32) + rf[j, 1].astype(F32)
            accb[j] = total.astype(BF16)
        else:
            total = combd[y].astype(F32) + rfd[0].astype(F32) + rfd[1].astype(F32)
            accbd[...] = total.astype(BF16)
        acc[j, : NZ * n, :] = total
        for d in (4, 3, 5, 2, 6, 1, 7):
            w_copy(j, d).start()

    def rs_last(j):
        n = rows_of(j)
        lo = j * R if j < CHUNKS else ROWS
        total = acc[j, pl.ds(pl.multiple_of(z * n, n), n), :]
        for d in range(1, NZ):
            w_copy(j, d).wait_recv()
            total = total + (rz[j, d] if j < CHUNKS else rzd[d]).astype(F32)
        mixed[lo : lo + n, :] = total

    for j in range(4):
        stats_wait(j)
        combine(j)
        for side in (0, 1):
            x_copy(j, side).start()
    for j in range(4):
        rs_second(j)
    for j in range(4):
        rs_third(j)
    for j in range(4):
        rs_last(j)

    total = mixed[...]
    inv_rms = lax.rsqrt(jnp.mean(total * total, axis=-1, keepdims=True) + EPS)
    out_ref[...] = (total * inv_rms * gain_ref[...] * OUT_SCALE).astype(BF16)

    for j in range(4):
        for d in range(1, NZ):
            z_copy(j, d).wait_send()
            w_copy(j, d).wait_send()
        for side in (0, 1):
            y_copy(j, side).wait_send()
            h_copy(j, side).wait_send()
            x_copy(j, side).wait_send()
            f_copy(j, side).wait_send()
        for yt in range(NY):

            @pl.when(STAT_Z[j] * NY + yt != me)
            def _():
                s_copy(j, yt).wait_send()

        @pl.when(z == STAT_Z[j])
        def _():
            @pl.loop(1, NKV)
            def _(d):
                r_copy(j, (me + d) % NKV).wait_send()


def attention(q, k, v, kp, vp, kd, vd, gain, prompt_len, step_lens, mix):
    vmem = pl.BlockSpec(memory_space=pltpu.VMEM)
    anyw = pl.BlockSpec(memory_space=pl.ANY)
    smem = pl.BlockSpec(memory_space=pltpu.SMEM)
    dma = pltpu.SemaphoreType.DMA
    V = pltpu.VMEM
    nt = CHUNKS * NY
    return pl.pallas_call(
        attend,
        out_shape=jax.ShapeDtypeStruct((PADDED, DV), BF16),
        in_specs=[vmem, vmem, vmem, anyw, anyw, anyw, anyw, vmem, smem, smem, smem],
        out_specs=vmem,
        scratch_shapes=[
            V((KEYS, 2 * DH), BF16),
            V((CACHE, DV), BF16),
            V((DV, KEYS), BF16),
            V((NKV, SEQC, 2 * DH), BF16),
            V((NKV, SEQC, DV), BF16),
            V((DV, NZ * SEQC), BF16),
            V((SEQC, 2 * DH), BF16),
            V((DV, SEQC), BF16),
            V((nt, TILE, 2 * DH), BF16),
            V((NY, TILED, 2 * DH), BF16),
            V((CACHE // 2, 128), F32),
            V((2, KEYS, TILE), F32),
            V((2, KEYS, TILE), BF16),
            V((nt, 2, DV, TILE), F32),
            V((NY, 2, DV, TILED), F32),
            V((nt + NY, 8, 128), F32),
            V((4, NKV, 8, 128), F32),
            V((4, 8, 128), F32),
            V((nt + NY, 8, 128), F32),
            V((nt, TILE, DV), BF16),
            V((NY, TILED, DV), BF16),
            V((CHUNKS, 2, TILE // 2, DV), BF16),
            V((2, TILED // 2, DV), BF16),
            V((CHUNKS, 2, TILE, DV), BF16),
            V((2, TILED, DV), BF16),
            V((4, TILE, DV), F32),
            V((CHUNKS, TILE, DV), BF16),
            V((TILED, DV), BF16),
            V((CHUNKS, NZ, R, DV), BF16),
            V((NZ, RD, DV), BF16),
            V((PADDED, DV), F32),
            dma((4,)),
            dma((4, NZ)), dma((4, NZ)),
            dma((4, 2)), dma((4, 2)),
            dma((4, 2)), dma((4, 2)),
            dma((4, NY)), dma((4, NKV)),
            dma((4, NKV)), dma((4, NY)),
            dma((4, 2)), dma((4, 2)),
            dma((4, 2)), dma((4, 2)),
            dma((4, NZ)), dma((4, NZ)),
        ],
        compiler_params=pltpu.CompilerParams(
            collective_id=0, has_side_effects=True, vmem_limit_bytes=60 << 20
        ),
        name="attend",
    )(q, k, v, kp, vp, kd, vd, gain, prompt_len, step_lens, mix)


def norm_rows(tokens, in_gain):
    floats = tokens.astype(F32)
    inv_rms = lax.rsqrt(jnp.mean(floats * floats, axis=-1, keepdims=True) + EPS)
    return (floats * inv_rms * in_gain).astype(BF16)


def project(normed, weight):
    flat_weight = weight.reshape(weight.shape[0], -1)
    return jnp.dot(normed, flat_weight, preferred_element_type=F32).astype(BF16)


def summed_on_arrival(shard, axis):
    count = lax.axis_size(axis)
    blocks = jnp.moveaxis(shard.reshape(shard.shape[0], count, -1), 1, 0)
    blocks = lax.all_to_all(blocks, axis, 0, 0, tiled=True)
    return jnp.sum(blocks.astype(F32), axis=0)


def on_device(
    piece_tokens, step_tokens, in_gain, w_query, w_key, w_value, w_out, mix_ratio, out_gain,
    prompt_keys, prompt_values, step_cache_keys, step_cache_values, prompt_len, step_lens,
):
    pad = jnp.zeros((RD - 1, piece_tokens.shape[1]), BF16)
    normed = norm_rows(jnp.concatenate([piece_tokens, step_tokens, pad], axis=0), in_gain)
    q = project(normed, w_query)
    k = project(normed, w_key)
    v = project(normed, w_value)
    headout = attention(
        q, k, v,
        prompt_keys.reshape(CACHE, 2 * DH), prompt_values.reshape(CACHE, DV),
        step_cache_keys.reshape(NKV, SEQC, 2 * DH), step_cache_values.reshape(NKV, SEQC, DV),
        out_gain.reshape(1, DV), prompt_len, step_lens, mix_ratio,
    )
    head_term = jnp.dot(
        headout[: ROWS + 1], w_out.reshape(-1, w_out.shape[-1]), preferred_element_type=F32
    ).astype(BF16)
    out = summed_on_arrival(head_term, "tp").astype(BF16)
    return (
        out[:ROWS], out[ROWS:],
        k[:ROWS].reshape(ROWS, 1, 2, DH), v[:ROWS].reshape(ROWS, 1, DV),
        k[ROWS : ROWS + 1].reshape(1, 1, 2, DH), v[ROWS : ROWS + 1].reshape(1, 1, DV),
    )


def solution(mesh):
    in_specs = (
        P("kv", None),
        P("kv", None),
        P(),
        P(None, "tp", None, None),
        P(None, "tp", None, None),
        P(None, "tp", None),
        P("tp", None, None),
        P("tp"),
        P(),
        P("kv", "tp", None, None),
        P("kv", "tp", None),
        P(None, "kv", "tp", None, None),
        P(None, "kv", "tp", None),
        P(),
        P(),
    )
    out_specs = (
        P("kv", "tp"),
        P("kv", "tp"),
        P("kv", "tp", None, None),
        P("kv", "tp", None),
        P("kv", "tp", None, None),
        P("kv", "tp", None),
    )
    return jax.shard_map(
        on_device, mesh=mesh, in_specs=in_specs, out_specs=out_specs, check_vma=False
    )
```

time: 336 us -> 128 us (0.38)
  waiting for transfers between devices: 120 us -> 10.5 us
  Pallas kernels: 0 us -> 82.7 us
  other arithmetic: 49.7 us -> 1.8 us
  matrix products: 44.8 us -> 6.93 us
  local copies, waits for them, and re-layouts: 44.8 us -> 11.1 us
  blocking collectives: 26.3 us -> 0 us
  starting transfers between devices: 32.7 us -> 12.5 us
  between operations: 15.9 us -> 2.08 us
    pallas_call x0 -> x1, Pallas kernels: none -> 82.7 us  [attention(): pl.pallas_call(attend, out_shape=jax.ShapeDtypeStruct((PADDED, DV), BF16)...]
    all_gather x1 -> x0, waiting for transfers between devices: 70.7 us -> none  [gather_together(): lines, at, outs = (lax.all_gather(ravelled, axis), 0, [])]
    all_to_all x4 -> x1, waiting for transfers between devices: 49.7 us -> 10.5 us  [summed_on_arrival(): blocks = lax.all_to_all(blocks, axis, 0, 0, tiled=True)]
    dot_general x18 -> x4, matrix products: 44.8 us -> 6.93 us  [the longest x3 5.66 us: project(): return jnp.dot(normed, flat_weight, preferred_element_type=F32).astype(BF16)]
    all_to_all x1 -> x0, blocking collectives: 26.3 us -> none  [summed_on_arrival(): blocks = lax.all_to_all(split_up(shard, dim, count), axis, 0, 0, tiled=True)]
    all_to_all x4 -> x1, starting transfers between devices: 32.6 us -> 12.5 us  [summed_on_arrival(): blocks = lax.all_to_all(blocks, axis, 0, 0, tiled=True)]
    unnamed x39 -> x20, local copies, waits for them, and re-layouts: 19.4 us -> 1.81 us
    concatenate x11 -> x0, other arithmetic: 14.6 us -> none  [the longest x6 12.3 us: piece_block(): jnp.concatenate([jnp.broadcast_to(cache_ok[None, :], (row_count, cache_ok...]
  transfers between devices with their start and end apart: 5 -> 1, of which waited for: 4 -> 1; matrix products, arithmetic and copies ran while one was open for 35% -> 2% of each run, Pallas kernels for 0% -> 0%
where the time goes in v1:
time: 128 us
  Pallas kernels  82.7 us (65%)
  starting transfers between devices  12.5 us (10%)
  local copies, waits for them, and re-layouts  11.1 us (9%)
  waiting for transfers between devices  10.5 us (8%)
  matrix products  6.93 us (5%)
  between operations  2.08 us (2%)
  other arithmetic  1.8 us (1%)
    pallas_call x1, Pallas kernels, attention(): pl.pallas_call(attend, out_shape=jax.ShapeDtypeStruct((PADDED, DV), BF16)...  82.7 us
    all_to_all x1, starting transfers between devices, summed_on_arrival(): blocks = lax.all_to_all(blocks, axis, 0, 0, tiled=True)  12.5 us
    all_to_all x1, waiting for transfers between devices, summed_on_arrival(): blocks = lax.all_to_all(blocks, axis, 0, 0, tiled=True)  10.5 us
    dot_general x3, matrix products, project(): return jnp.dot(normed, flat_weight, preferred_element_type=F32).astype(BF16)  5.66 us
    reshape x1, local copies, waits for them, and re-layouts, on_device(): step_cache_keys.reshape(NKV, SEQC, 2 * DH)  4.45 us
  transfers between devices with their start and end apart: 1, of which 1 were waited for; matrix products, arithmetic and copies ran while one was open for 2% of the time, Pallas kernels for 0%

profile of v1, /device:TPU:1, one launch (start us, length us, event | category | flops | bytes accessed | tf_op | source)
XLA Modules:
  0.0 127.6 jit_solution(9043842612471843488)
XLA Ops:
  0.6 0.0 copy-start
  0.7 0.1 pad.2.clone
  0.7 1.7 %fusion.9 = f32[112]{0:T(128)S(1)} fusion(bf16[1,4096]{1,0:T(2,128)(2,1)} %param.16, bf16[96,4096]{1,0:T(8,128)(2,1)} %param.15, bf16[112]{0:T(256)(128)(2,1)S(1)} %pad.2.clone), kind=kLoop, calls=%fused_computation.12 | loop fusion | flops 3669904 | bytes 795296 | tf_op jit(solution)/shard_map/reduce_sum | solution.py:462
  2.4 0.0 copy-start.2
  2.4 0.0 copy-start.5
  2.4 0.0 copy-start.6
  2.5 0.0 copy-start.8
  2.5 3.1 %fusion.12.v_own = bf16[112,256]{1,0:T(8,128)(2,1)} fusion(bf16[4096,1,256]{2,0,1:T(8,128)(2,1)} %param.20, f32[4096]{0:T(1024)} %param.17, f32[112]{0:T(128)S(1)} %add_rsqrt_fusion, bf16[1,4096]{1,0:T(2,128)(2,1)} %param.16, bf16[96,4096]{1,0:T(8,128)(2,1)} %param.15, bf16[112]{0:T(256)(128)(2,1)S(1)} %pad.2.clone), kind=kOutput, calls=%fused_computation.15 | convolution fusion | flops 239038464 | bytes 2966176 | tf_op jit(solution)/shard_map/dot_general | solution.py:468
  5.6 0.0 copy-done.2
  5.6 0.0 copy-done.5
  5.6 0.0 copy-done.6
  5.6 0.0 copy-done.8
  5.6 0.0 copy-start.7
  5.7 1.3 fusion.18.k_own
  6.9 0.3 copy-done.7
  7.2 1.3 fusion.15.q_own
  8.5 0.0 copy-start.1
  8.5 4.5 %reshape.68.kd_hbm = bf16[32,128,256]{2,1,0:T(8,128)(2,1)} reshape(bf16[32,128,1,2,128]{4,3,2,1,0:T(2,128)(2,1)} %param.26) | data formatting | bytes 4194304 | tf_op jit(solution)/shard_map/reshape | solution.py:490
  12.9 0.0 copy-done.1
  13.0 1.1 copy.42
  15.4 82.7 %attend.1 = bf16[112,256]{1,0:T(8,128)(2,1)} custom-call(bf16[112,256]{1,0:T(8,128)(2,1)} %fusion.15.q_own, bf16[112,256]{1,0:T(8,128)(2,1)} %fusion.18.k_own, bf16[112,256]{1,0:T(8,128)(2,1)} %fusion.12.v_own, bf16[2048,256]{1,0:T(8,128)(2,1)} %bitcast.42, bf16[2048,256]{1,0:T(8,128)(2,1)} %bitcast.47, bf16[32,128,256]{2,1,0:T(8,128)(2,1)} %reshape.68.kd_hbm, ...), custom_call_target="tpu_custom_call" | custom-call | tf_op jit(solution)/shard_map/attend/pallas_call | solution.py:406
  98.0 0.0 copy-done
  98.1 1.3 convolution_convert_fusion
  99.3 0.3 copy.27
  99.6 0.1 slice.34
  99.7 0.0 slice-start
  99.7 0.0 copy-start.4
  99.7 0.0 copy-start.3
  99.7 1.1 copy.43
  100.9 12.5 %all-to-all-start = ((bf16[8,97,512]{2,1,0:T(8,128)(2,1)}), bf16[8,97,512]{2,1,0:T(8,128)(2,1)S(1)}, u32[]{:S(2)}, u32[]{:S(2)}) async-start(bf16[8,97,512]{2,1,0:T(8,128)(2,1)} %bitcast.43), calls=%async_computation | async-start | bytes 1703936 | tf_op jit(solution)/shard_map/all_to_all | solution.py:474
  113.4 0.0 slice-done
  113.4 0.6 reshape.73
  114.1 0.0 copy-done.4
  114.1 0.5 slice_reduce_fusion
  114.6 0.0 copy-done.3
  114.6 0.6 slice_bitcast_fusion.1
  115.2 0.6 slice_bitcast_fusion
  115.8 10.5 %all-to-all-done = bf16[8,97,512]{2,1,0:T(8,128)(2,1)S(1)} async-done(((bf16[8,97,512]{2,1,0:T(8,128)(2,1)}), bf16[8,97,512]{2,1,0:T(8,128)(2,1)S(1)}, u32[]{:S(2)}, u32[]{:S(2)}) %all-to-all-start) | async-done | bytes 794656 | tf_op jit(solution)/shard_map/all_to_all | solution.py:474
  126.3 0.1 reduce_sum.22
  126.4 0.6 slice.28
  127.1 0.6 slice.29
  (2 shorter events, 0.0 us)
Async XLA Ops:
  0.6 97.4 %copy-start = (bf16[1,256,4096]{2,1,0:T(8,128)(2,1)S(1)}, bf16[1,256,4096]{2,1,0:T(8,128)(2,1)}, u32[]{:S(2)}) copy-start(bf16[1,256,4096]{2,1,0:T(8,128)(2,1)} %param.21) | copy-start | bytes 6291460
  2.4 3.2 %copy-start.2 = (bf16[96,4096]{1,0:T(8,128)(2,1)S(1)}, bf16[96,4096]{1,0:T(8,128)(2,1)}, u32[]{:S(2)}) copy-start(bf16[96,4096]{1,0:T(8,128)(2,1)} %param.15) | copy-start | bytes 2359300
  2.4 3.2 %copy-start.5 = (bf16[1,4096]{1,0:T(2,128)(2,1)S(1)}, bf16[1,4096]{1,0:T(2,128)(2,1)}, u32[]{:S(2)}) copy-start(bf16[1,4096]{1,0:T(2,128)(2,1)} %param.16) | copy-start | bytes 24580
  2.4 3.2 %copy-start.6 = (bf16[4096,1,2,128]{3,2,1,0:T(2,128)(2,1)S(1)}, bf16[4096,1,2,128]{3,2,1,0:T(2,128)(2,1)}, u32[]{:S(2)}) copy-start(bf16[4096,1,2,128]{3,2,1,0:T(2,128)(2,1)} %param.19) | copy-start | bytes 6291460
  2.5 3.2 %copy-start.8 = (f32[4096]{0:T(1024)S(1)}, f32[4096]{0:T(1024)}, u32[]{:S(2)}) copy-start(f32[4096]{0:T(1024)} %param.17) | copy-start | bytes 49156
  5.6 1.6 %copy-start.7 = (bf16[4096,1,2,128]{3,2,1,0:T(2,128)(2,1)S(1)}, bf16[4096,1,2,128]{3,2,1,0:T(2,128)(2,1)}, u32[]{:S(2)}) copy-start(bf16[4096,1,2,128]{3,2,1,0:T(2,128)(2,1)} %param.18) | copy-start | bytes 6291460
  8.5 4.5 %copy-start.1 = (bf16[2048,1,2,128]{3,2,1,0:T(2,128)(2,1)S(1)}, bf16[2048,1,2,128]{3,2,1,0:T(2,128)(2,1)}, u32[]{:S(2)}) copy-start(bf16[2048,1,2,128]{3,2,1,0:T(2,128)(2,1)} %param.24) | copy-start | bytes 3145732
  99.7 13.7 %slice-start = ((bf16[112,256]{1,0:T(8,128)(2,1)}), bf16[96,256]{1,0:T(8,128)(2,1)S(1)}, s32[]{:S(2)}) async-start(bf16[112,256]{1,0:T(8,128)(2,1)} %fusion.18.k_own), calls=%async_computation.1 | async-start | bytes 98304 | tf_op jit(solution)/shard_map/slice | solution.py:499
  99.7 14.4 %copy-start.4 = (bf16[112,256]{1,0:T(8,128)(2,1)S(1)}, bf16[112,256]{1,0:T(8,128)(2,1)}, u32[]{:S(2)}) copy-start(bf16[112,256]{1,0:T(8,128)(2,1)} %fusion.18.k_own) | copy-start | bytes 172036
  99.7 14.9 %copy-start.3 = (bf16[112,256]{1,0:T(8,128)(2,1)S(1)}, bf16[112,256]{1,0:T(8,128)(2,1)}, u32[]{:S(2)}) copy-start(bf16[112,256]{1,0:T(8,128)(2,1)} %fusion.12.v_own) | copy-start | bytes 172036
  100.9 25.4 %all-to-all-start = ((bf16[8,97,512]{2,1,0:T(8,128)(2,1)}), bf16[8,97,512]{2,1,0:T(8,128)(2,1)S(1)}, u32[]{:S(2)}, u32[]{:S(2)}) async-start(bf16[8,97,512]{2,1,0:T(8,128)(2,1)} %bitcast.43), calls=%async_computation | async-start | bytes 1703936 | tf_op jit(solution)/shard_map/all_to_all | solution.py:474

commit v2 on v1

v2 whole, which is shorter than its diff:
```python
import functools
import math

import jax
import jax.numpy as jnp
from jax import lax
from jax.experimental import pallas as pl
from jax.experimental.pallas import tpu as pltpu
from jax.sharding import PartitionSpec as P

EPS = 1e-06
OUT_SCALE = 0.8
NZ, NY, NKV, NX = 8, 4, 32, 4
D, OUTB = 4096, 512
ROWS = 96
CHUNKS = 3
R = ROWS // CHUNKS
RD = 16
TILE = NZ * R
TILED = NZ * RD
CACHE = 2048
KEYS = CACHE + 128
SEQC = 128
DH, DV = 128, 256
PADDED = ROWS + RD
EXPC = DH ** (-0.5) * math.log2(math.e)
STAT_Z = (1, 4, 7)
F32, BF16 = jnp.float32, jnp.bfloat16
NT = (((1,), (1,)), ((), ()))


def attend(
    q_own, k_own, normed, wv_hbm, kp_hbm, vp_hbm, kd_hbm, vd_hbm, wo_hbm, gain_ref, plen, slens, mix,
    piece_ref, step_ref, pv_ref, sv_ref,
    wv, wo, kraw, kfloat, kbuf, vnat, vt, kd, vdn, vtd, ksd, vse, qall, qd, bias, sbuf, pbuf, oacc,
    stat, srecv, ressend, res, dsend, drecv, comb, rh, rf, acc, accb, rz, mixed,
    term, tsum, pr, th, tf,
    load_sem, zs, zr, ys, yr, hs, hr, ss, sr, rs, rr, xs, xr, fs, fr, ws, wr, ds, dr,
    ps, ps_r, ts, tr, us, ur,
):
    me = lax.axis_index("kv")
    tp = lax.axis_index("tp")
    z = me // NY
    y = me % NY
    yp, ym, y2 = (y + 1) % NY, (y + 3) % NY, (y + 2) % NY
    x = tp // 2
    core = tp % 2
    xp, xm, x2 = (x + 1) % NX, (x + 3) % NX, (x + 2) % NX

    def at_kv(index):
        return {"kv": index}

    def rcopy(src, dst, s_sem, r_sem, target):
        return pltpu.make_async_remote_copy(
            src_ref=src, dst_ref=dst, send_sem=s_sem, recv_sem=r_sem,
            device_id=at_kv(target), device_id_type=pl.DeviceIdType.MESH,
        )

    def tcopy(src, dst, s_sem, r_sem, tx, tc):
        return pltpu.make_async_remote_copy(
            src_ref=src, dst_ref=dst, send_sem=s_sem, recv_sem=r_sem,
            device_id={"tp": tx * 2 + tc}, device_id_type=pl.DeviceIdType.MESH,
        )

    def rows_of(j):
        return R if j < CHUNKS else RD

    def qtile(j, yy):
        return qall.at[j * NY + yy] if j < CHUNKS else qd.at[yy]

    def ctile(j, yy):
        return comb.at[j * NY + yy]

    def zblock(view, zz, n):
        return view.at[pl.ds(pl.multiple_of(zz * n, n), n), :]

    barrier = pltpu.get_barrier_semaphore()

    @pl.loop(1, NKV)
    def _(d):
        pl.semaphore_signal(
            barrier, inc=1, device_id=at_kv((me + d) % NKV),
            device_id_type=pl.DeviceIdType.MESH,
        )

    for tx, tc in ((x, 1 - core), (xp, core), (xm, core)):
        pl.semaphore_signal(
            barrier, inc=1, device_id={"tp": tx * 2 + tc}, device_id_type=pl.DeviceIdType.MESH
        )

    loads = [
        pltpu.make_async_copy(wv_hbm, wv, load_sem.at[0]),
        pltpu.make_async_copy(kp_hbm, kraw.at[pl.ds(0, 2 * CACHE), :], load_sem.at[1]),
        pltpu.make_async_copy(vp_hbm, vnat, load_sem.at[2]),
        pltpu.make_async_copy(kd_hbm, kraw.at[pl.ds(2 * CACHE, 2 * NKV * SEQC), :], load_sem.at[3]),
        pltpu.make_async_copy(vd_hbm, vdn, load_sem.at[4]),
        pltpu.make_async_copy(wo_hbm, wo, load_sem.at[5]),
    ]
    for load in loads:
        load.start()

    for j in range(4):
        n = rows_of(j)
        lo = j * R if j < CHUNKS else ROWS
        mine = qtile(j, y)
        mine[pl.ds(pl.multiple_of(z * n, n), n), :] = q_own[lo : lo + n, :]

    pl.semaphore_wait(barrier, NKV - 1 + 3)

    def z_copy(j, d):
        n = rows_of(j)
        zt = (z + d) % NZ
        block = zblock(qtile(j, y), z, n)
        return rcopy(block, block, zs.at[j], zr.at[j], zt * NY + y)

    def z_all(j):
        some = qtile(j, y).at[pl.ds(0, (NZ - 1) * rows_of(j)), :]
        return rcopy(some, some, zs.at[j], zr.at[j], z * NY + yp)

    for j in range(4):
        for d in (1, 7, 2, 6, 3, 5, 4):
            z_copy(j, d).start()

    loads[0].wait()
    values = jnp.dot(normed[...], wv[...], preferred_element_type=F32).astype(BF16)
    pv_ref[...] = values[:ROWS, :]
    sv_ref[...] = values[ROWS : ROWS + 1, :]
    kbuf[CACHE : CACHE + ROWS, :] = k_own[:ROWS, :]
    kbuf[CACHE + ROWS :, :] = jnp.zeros((KEYS - CACHE - ROWS, 2 * DH), BF16)
    ksd[:RD, :] = k_own[ROWS:, :]
    ksd[RD:, :] = jnp.zeros((SEQC - RD, 2 * DH), BF16)
    tail = jnp.concatenate([values[:ROWS, :], jnp.zeros((128 - ROWS, DV), BF16)], axis=0)
    vt[:, CACHE:] = tail.T
    tail = jnp.concatenate([values[ROWS:, :], jnp.zeros((128 - RD, DV), BF16)], axis=0)
    vse[...] = tail.T
    half = CACHE // 2
    place = me * CACHE + half + lax.broadcasted_iota(jnp.int32, (half, 128), 0)
    bias[...] = jnp.where(place < plen[0], 0.0, -jnp.inf).astype(F32)
    mixed[...] = jnp.zeros((PADDED, DV), F32)
    loads[1].wait()
    loads[2].wait()

    @pl.loop(0, CACHE // 256)
    def _(b):
        kfloat[...] = kraw[pl.ds(pl.multiple_of(b * 512, 512), 512), :].astype(F32)
        rows = pl.ds(pl.multiple_of(b * 256, 256), 256)
        for c in range(2):
            kbuf[rows, c * DH : (c + 1) * DH] = kfloat[pl.ds(c, 256, 2), :].astype(BF16)

    for b in range(CACHE // 256):
        vt[:, b * 256 : (b + 1) * 256] = vnat[b * 256 : (b + 1) * 256, :].T
    loads[3].wait()

    @pl.loop(0, NKV // 2)
    def _(b):
        kfloat[...] = kraw[pl.ds(pl.multiple_of(2 * CACHE + b * 512, 512), 512), :].astype(F32)
        for c in range(2):
            flat = kfloat[pl.ds(c, 256, 2), :].astype(BF16)
            for s in range(2):
                kd[2 * b + s, :, c * DH : (c + 1) * DH] = flat[s * SEQC : (s + 1) * SEQC]

    def z_wait_y_send(j):
        z_all(j).wait_recv()
        y_copy(j, 0).start()
        y_copy(j, 1).start()

    def y_copy(j, side):
        tile = qtile(j, y)
        return rcopy(tile, tile, ys.at[j, side], yr.at[j, side], z * NY + (yp if side == 0 else ym))

    def half_of(view, j, side):
        h = NZ * rows_of(j) // 2
        return view.at[pl.ds(side * h, h), :]

    def h_copy(j, side):
        part = half_of(qtile(j, ym if side == 0 else yp), j, side)
        return rcopy(part, part, hs.at[j, side], hr.at[j, side], z * NY + (yp if side == 0 else ym))

    def y_wait_fwd(j):
        for side in (0, 1):
            tile = qtile(j, ym if side == 0 else yp)
            rcopy(tile, tile, ys.at[j, side], yr.at[j, side], z * NY + yp).wait_recv()
            h_copy(j, side).start()

    def h_wait(j):
        for side in (0, 1):
            part = half_of(qtile(j, y2), j, side)
            rcopy(part, part, hs.at[j, side], hr.at[j, side], z * NY + yp).wait_recv()

    def s_copy(j, yt):
        return rcopy(
            stat.at[j * NY + yt], srecv.at[j, me], ss.at[j, yt], sr.at[j], STAT_Z[j] * NY + yt
        )

    def stats_send(j):
        for yt in range(NY):
            target = STAT_Z[j] * NY + yt

            @pl.when(target != me)
            def _():
                s_copy(j, yt).start()

            @pl.when(target == me)
            def _():
                srecv[j, me] = stat[j * NY + yt]

    def r_copy(j, target):
        return rcopy(ressend.at[j], res.at[j * NY + y], rs.at[j], rr.at[j, y], target)

    def stats_own(j):
        @pl.when(z == STAT_Z[j])
        def _():
            most = srecv.at[j, pl.ds(0, NKV - 1)]
            rcopy(most, most, rs.at[j], sr.at[j], z * NY + yp).wait_recv()
            every = srecv[j]
            best = jnp.max(every[:, 0:4, :], axis=0)
            norm = jnp.sum(every[:, 4:8, :] * jnp.exp2((every[:, 0:4, :] - best[None]) * EXPC), axis=0)
            both = jnp.concatenate([best, 1.0 / norm], axis=0)
            ressend[j] = both
            res[j * NY + y] = both

            @pl.loop(1, NKV)
            def _(d):
                r_copy(j, (me + d) % NKV).start()

    def stats_wait(j):
        for yt in range(NY):
            owner = STAT_Z[j] * NY + yt

            @pl.when(owner != me)
            def _():
                rcopy(ressend.at[j], res.at[j * NY + yt], rs.at[j], rr.at[j, yt], owner).wait_recv()

    def combine(j):
        @pl.loop(0, NY)
        def _(yy):
            tt = j * NY + yy
            factors = []
            for c in range(2):
                pick = lambda ref, lo: jnp.concatenate(
                    [ref[tt, lo + 2 * c + hh : lo + 2 * c + hh + 1, :] for hh in range(2)], axis=1
                )
                factors.append(jnp.exp2((pick(stat, 0) - pick(res, 0)) * EXPC) * pick(res, 4))
            both = oacc[tt, 0] * factors[0] - oacc[tt, 1] * (factors[1] * mix[0])
            comb[tt] = both.T.astype(BF16)

    def x_copy(j, side):
        part = half_of(ctile(j, y2), j, side)
        return rcopy(part, rh.at[j, side], xs.at[j, side], xr.at[j, side], z * NY + (yp if side == 0 else ym))

    def f_copy(j, side):
        tile = ctile(j, yp if side == 0 else ym)
        return rcopy(tile, rf.at[j, side], fs.at[j, side], fr.at[j, side], z * NY + (yp if side == 0 else ym))

    def rs_first(j):
        stats_wait(j)
        combine(j)
        for side in (0, 1):
            x_copy(j, side).start()

    def rs_second(j):
        for side in (0, 1):
            x_copy(j, side).wait_recv()
            part = half_of(ctile(j, yp if side == 0 else ym), j, side)
            part[...] = (part[...].astype(F32) + rh[j, side].astype(F32)).astype(BF16)
            f_copy(j, side).start()

    def w_copy(j, d):
        zt = (z + d) % NZ
        return rcopy(zblock(accb.at[j], zt, R), rz.at[j, d - 1], ws.at[j], wr.at[j], zt * NY + y)

    def w_all(j):
        return rcopy(rz.at[j], rz.at[j], ws.at[j], wr.at[j], z * NY + yp)

    def rs_third(j):
        for side in (0, 1):
            f_copy(j, side).wait_recv()
        total = comb[j * NY + y].astype(F32) + rf[j, 0].astype(F32) + rf[j, 1].astype(F32)
        accb[j] = total.astype(BF16)
        acc[j] = total
        for d in (4, 3, 5, 2, 6, 1, 7):
            w_copy(j, d).start()

    def rs_last(j):
        total = acc[j, pl.ds(pl.multiple_of(z * R, R), R), :]
        w_all(j).wait_recv()
        for d in range(NZ - 1):
            total = total + rz[j, d].astype(F32)
        mixed[j * R : (j + 1) * R, :] = total

    def span(j):
        return slice(j * R, j * R + rows_of(j))

    def p_copy(j):
        return tcopy(
            term.at[1 - core, :, span(j), :], pr.at[:, span(j), :], ps.at[j], ps_r.at[j], x, 1 - core
        )

    def project_out(j):
        n = rows_of(j)
        total = mixed[span(j), :]
        inv_rms = lax.rsqrt(jnp.mean(total * total, axis=-1, keepdims=True) + EPS)
        head = (total * inv_rms * gain_ref[...] * OUT_SCALE).astype(BF16)
        for tx in range(NX):
            for tc in range(2):
                at = (tx * 2 + tc) * OUTB
                one = jnp.dot(head, wo[:, at : at + OUTB], preferred_element_type=F32)
                term[tc, tx, span(j), :] = one.astype(BF16)
        p_copy(j).start()

    def t_copy(j, side):
        cols = slice(side * OUTB // 2, (side + 1) * OUTB // 2)
        return tcopy(
            tsum.at[x2, span(j), cols], th.at[side, span(j), :], ts.at[j, side], tr.at[j, side],
            xp if side == 0 else xm, core,
        )

    def u_copy(j, side):
        to = xp if side == 0 else xm
        return tcopy(tsum.at[to, span(j), :], tf.at[side, span(j), :], us.at[j, side], ur.at[j, side], to, core)

    def tp_first(j):
        p_copy(j).wait_recv()
        for tx in range(NX):
            both = term[core, tx, span(j), :].astype(F32) + pr[tx, span(j), :].astype(F32)
            tsum[tx, span(j), :] = both.astype(BF16)
        for side in (0, 1):
            t_copy(j, side).start()

    def tp_second(j):
        for side in (0, 1):
            t_copy(j, side).wait_recv()
            to = xp if side == 0 else xm
            cols = slice(side * OUTB // 2, (side + 1) * OUTB // 2)
            both = tsum[to, span(j), cols].astype(F32) + th[side, span(j), :].astype(F32)
            tsum[to, span(j), cols] = both.astype(BF16)
            u_copy(j, side).start()

    def tp_last(j):
        for side in (0, 1):
            u_copy(j, side).wait_recv()
        own = term[core, x, span(j), :].astype(F32) + pr[x, span(j), :].astype(F32)
        total = (own + tf[0, span(j), :].astype(F32) + tf[1, span(j), :].astype(F32)).astype(BF16)
        if j < CHUNKS:
            piece_ref[span(j), :] = total
        else:
            step_ref[...] = total[:1]

    KB = [(b * 256, 256) for b in range(CACHE // 256)] + [(CACHE, 128)]

    @pl.loop(0, CHUNKS * NY)
    def _(t):
        for step, work, arg in (
            (0, z_wait_y_send, 0),
            (1, z_wait_y_send, 1),
            (1, y_wait_fwd, 0),
            (2, z_wait_y_send, 2),
            (3, h_wait, 0),
            (3, z_wait_y_send, 3),
            (4, stats_send, 0),
            (4, y_wait_fwd, 1),
            (5, y_wait_fwd, 2),
            (6, y_wait_fwd, 3),
            (7, h_wait, 1),
            (7, stats_own, 0),
            (8, stats_send, 1),
            (10, rs_first, 0),
            (11, h_wait, 2),
            (11, stats_own, 1),
            (11, rs_second, 0),
        ):
            pl.when(t == step)(functools.partial(work, arg))

        j = t // NY
        i = t % NY
        yy = (y + jnp.where(i == 2, 3, jnp.where(i == 3, 2, i))) % NY
        tt = j * NY + yy
        lane = lax.broadcasted_iota(jnp.int32, (128, TILE), 1)
        row = lax.broadcasted_iota(jnp.int32, (128, TILE), 0)
        row_place = ((lane // R) * NY + yy) * ROWS + R * j + lane % R
        fresh_ok = (row < ROWS) & (me * ROWS + row <= row_place)
        for c in range(2):
            cols = slice(c * DH, (c + 1) * DH)
            q = qall[tt, :, cols]
            top = jnp.full((8, TILE), -jnp.inf, F32)
            for at, size in KB:
                s = lax.dot_general(kbuf[at : at + size, cols], q, NT, preferred_element_type=F32)
                if at == CACHE:
                    s = jnp.where(fresh_ok, s, -jnp.inf)
                elif at >= half:
                    b = bias[at - half : at - half + size, :]
                    s = s + jnp.concatenate([b, b], axis=1)
                sbuf[c, at : at + size, :] = s
                top = jnp.maximum(top, jnp.max(s.reshape(size // 8, 8, TILE), axis=0))
            m = jnp.max(top, axis=0, keepdims=True)
            total = jnp.zeros((8, TILE), F32)
            for at, size in KB:
                w = jnp.exp2((sbuf[c, at : at + size, :] - m) * EXPC)
                total = total + jnp.sum(w.reshape(size // 8, 8, TILE), axis=0)
                pbuf[c, at : at + size, :] = w.astype(BF16)
            total = jnp.sum(total, axis=0, keepdims=True)
            oacc[tt, c] = jnp.dot(vt[...], pbuf[c], preferred_element_type=F32)
            for hh in range(2):
                stat[tt, 2 * c + hh : 2 * c + hh + 1, :] = m[:, hh * 128 : (hh + 1) * 128]
                stat[tt, 4 + 2 * c + hh : 5 + 2 * c + hh, :] = total[:, hh * 128 : (hh + 1) * 128]

    stats_send(2)

    loads[4].wait()
    h_wait(3)

    @pl.loop(0, NY)
    def _(yy):
        q2 = qd[yy]
        lane = lax.broadcasted_iota(jnp.int32, (SEQC, TILED), 1)
        row = lax.broadcasted_iota(jnp.int32, (SEQC, TILED), 0)
        own = (lane // RD == jnp.where(yy == y, z, NZ)) & (row == 0)
        limit = jnp.zeros((SEQC, TILED), jnp.int32)
        for zz in range(NZ):
            vtd[:, zz * SEQC : (zz + 1) * SEQC] = vdn[zz * NY + yy].T
            limit = jnp.where(lane // RD == zz, slens[zz * NY + yy], limit)
        seen = me * SEQC + row < limit
        for c in range(2):
            cols = slice(c * DH, (c + 1) * DH)
            q = q2[:, cols]
            s = jnp.full((SEQC, TILED), -jnp.inf, F32)
            for zz in range(NZ):
                one = lax.dot_general(kd[zz * NY + yy, :, cols], q, NT, preferred_element_type=F32)
                s = jnp.where((lane // RD == zz) & seen, one, s)
            extra = lax.dot_general(ksd[:, cols], q, NT, preferred_element_type=F32)
            extra = jnp.where(own, extra, -jnp.inf)
            m = jnp.max(jnp.maximum(s, extra), axis=0, keepdims=True)
            w = jnp.exp2((s - m) * EXPC)
            we = jnp.exp2((extra - m) * EXPC)
            total = jnp.sum(w + we, axis=0, keepdims=True)
            out = jnp.dot(vse[...], we.astype(BF16), preferred_element_type=F32)
            for zz in range(NZ):
                part = jnp.where(lane // RD == zz, w, 0.0).astype(BF16)
                out = out + jnp.dot(
                    vtd[:, zz * SEQC : (zz + 1) * SEQC], part, preferred_element_type=F32
                )
            out = out.T
            for zz in range(NZ):
                b = zz * NY + yy
                for hh in range(2):
                    dsend[b, 2 * c + hh : 2 * c + hh + 1, :] = out[
                        RD * zz : RD * zz + 1, hh * 128 : (hh + 1) * 128
                    ]
                dsend[b, 4 + c : 5 + c, :] = m
                dsend[b, 6 + c : 7 + c, :] = total

    def d_copy(target):
        return rcopy(dsend.at[target], drecv.at[me], ds.at[0], dr.at[0], target)

    @pl.loop(1, NKV)
    def _(d):
        d_copy((me + d) % NKV).start()

    drecv[me] = dsend[me]

    def d_all():
        most = drecv.at[pl.ds(0, NKV - 1)]
        return rcopy(most, most, ds.at[0], dr.at[0], z * NY + yp)

    def decode_row():
        d_all().wait_recv()
        mine = lax.broadcasted_iota(jnp.int32, (NKV, 128), 1) == RD * z
        parts = []
        for c in range(2):
            pick = lambda at: jnp.sum(jnp.where(mine, drecv[:, at, :], 0.0), axis=1, keepdims=True)
            m = pick(4 + c)
            scale = jnp.exp2((m - jnp.max(m, axis=0, keepdims=True)) * EXPC)
            norm = jnp.sum(pick(6 + c) * scale, axis=0, keepdims=True)
            parts.append(
                [jnp.sum(drecv[:, 2 * c + hh, :] * scale, axis=0, keepdims=True) / norm for hh in range(2)]
            )
        for hh in range(2):
            mixed[ROWS : ROWS + 1, hh * 128 : (hh + 1) * 128] = parts[0][hh] - mix[0] * parts[1][hh]

    rs_third(0)
    rs_first(1)
    stats_own(2)
    rs_second(1)
    rs_last(0)
    loads[5].wait()
    project_out(0)
    rs_third(1)
    rs_first(2)
    tp_first(0)
    rs_last(1)
    project_out(1)
    rs_second(2)
    tp_second(0)
    decode_row()
    project_out(3)
    rs_third(2)
    tp_first(1)
    tp_last(0)
    tp_first(3)
    tp_second(1)
    tp_second(3)
    rs_last(2)
    project_out(2)
    tp_last(1)
    tp_last(3)
    tp_first(2)
    tp_second(2)
    tp_last(2)

    for j in range(4):
        z_all(j).wait_send()
        p_copy(j).wait_send()
        for side in (0, 1):
            y_copy(j, side).wait_send()
            h_copy(j, side).wait_send()
            t_copy(j, side).wait_send()
            u_copy(j, side).wait_send()
    for j in range(CHUNKS):
        w_all(j).wait_send()
        for side in (0, 1):
            x_copy(j, side).wait_send()
            f_copy(j, side).wait_send()
        for yt in range(NY):

            @pl.when(STAT_Z[j] * NY + yt != me)
            def _():
                s_copy(j, yt).wait_send()

        @pl.when(z == STAT_Z[j])
        def _():
            most = srecv.at[j, pl.ds(0, NKV - 1)]
            rcopy(most, most, rs.at[j], sr.at[j], z * NY + yp).wait_send()

    d_all().wait_send()


def attention(q, k, normed, wv, kp, vp, kd, vd, wo, gain, prompt_len, step_lens, mix):
    vmem = pl.BlockSpec(memory_space=pltpu.VMEM)
    anyw = pl.BlockSpec(memory_space=pl.ANY)
    smem = pl.BlockSpec(memory_space=pltpu.SMEM)
    dma = pltpu.SemaphoreType.DMA
    V = pltpu.VMEM
    nt = CHUNKS * NY
    return pl.pallas_call(
        attend,
        out_shape=(
            jax.ShapeDtypeStruct((ROWS, OUTB), BF16),
            jax.ShapeDtypeStruct((1, OUTB), BF16),
            jax.ShapeDtypeStruct((ROWS, DV), BF16),
            jax.ShapeDtypeStruct((1, DV), BF16),
        ),
        in_specs=[vmem, vmem, vmem] + [anyw] * 6 + [vmem, smem, smem, smem],
        out_specs=(vmem,) * 4,
        scratch_shapes=[
            V((D, DV), BF16),
            V((DV, D), BF16),
            V((2 * CACHE + 2 * NKV * SEQC, DH), BF16),
            V((512, DH), F32),
            V((KEYS, 2 * DH), BF16),
            V((CACHE, DV), BF16),
            V((DV, KEYS), BF16),
            V((NKV, SEQC, 2 * DH), BF16),
            V((NKV, SEQC, DV), BF16),
            V((DV, NZ * SEQC), BF16),
            V((SEQC, 2 * DH), BF16),
            V((DV, SEQC), BF16),
            V((nt, TILE, 2 * DH), BF16),
            V((NY, TILED, 2 * DH), BF16),
            V((CACHE // 2, 128), F32),
            V((2, KEYS, TILE), F32),
            V((2, KEYS, TILE), BF16),
            V((nt, 2, DV, TILE), F32),
            V((nt, 8, 128), F32),
            V((CHUNKS, NKV, 8, 128), F32),
            V((CHUNKS, 8, 128), F32),
            V((nt, 8, 128), F32),
            V((NKV, 8, 128), F32),
            V((NKV, 8, 128), F32),
            V((nt, TILE, DV), BF16),
            V((CHUNKS, 2, TILE // 2, DV), BF16),
            V((CHUNKS, 2, TILE, DV), BF16),
            V((CHUNKS, TILE, DV), F32),
            V((CHUNKS, TILE, DV), BF16),
            V((CHUNKS, NZ - 1, R, DV), BF16),
            V((PADDED, DV), F32),
            V((2, NX, PADDED, OUTB), BF16),
            V((NX, PADDED, OUTB), BF16),
            V((NX, PADDED, OUTB), BF16),
            V((2, PADDED, OUTB // 2), BF16),
            V((2, PADDED, OUTB), BF16),
            dma((6,)),
            dma((4,)), dma((4,)),
            dma((4, 2)), dma((4, 2)),
            dma((4, 2)), dma((4, 2)),
            dma((3, NY)), dma((3,)),
            dma((3,)), dma((3, NY)),
            dma((3, 2)), dma((3, 2)),
            dma((3, 2)), dma((3, 2)),
            dma((3,)), dma((3,)),
            dma((1,)), dma((1,)),
            dma((4,)), dma((4,)),
            dma((4, 2)), dma((4, 2)),
            dma((4, 2)), dma((4, 2)),
        ],
        compiler_params=pltpu.CompilerParams(
            collective_id=0, has_side_effects=True, vmem_limit_bytes=62 << 20
        ),
        name="attend",
    )(q, k, normed, wv, kp, vp, kd, vd, wo, gain, prompt_len, step_lens, mix)


def norm_rows(tokens, in_gain):
    floats = tokens.astype(F32)
    inv_rms = lax.rsqrt(jnp.mean(floats * floats, axis=-1, keepdims=True) + EPS)
    return (floats * inv_rms * in_gain).astype(BF16)


def project(normed, weight):
    flat_weight = weight.reshape(weight.shape[0], -1)
    return jnp.dot(normed, flat_weight, preferred_element_type=F32).astype(BF16)


def on_device(
    piece_tokens, step_tokens, in_gain, w_query, w_key, w_value, w_out, mix_ratio, out_gain,
    prompt_keys, prompt_values, step_cache_keys, step_cache_values, prompt_len, step_lens,
):
    pad = jnp.zeros((RD - 1, piece_tokens.shape[1]), BF16)
    normed = norm_rows(jnp.concatenate([piece_tokens, step_tokens, pad], axis=0), in_gain)
    q = project(normed, w_query)
    k = project(normed, w_key)
    piece_out, step_out, piece_v, step_v = attention(
        q, k, normed, w_value.reshape(D, DV),
        prompt_keys.reshape(2 * CACHE, DH), prompt_values.reshape(CACHE, DV),
        step_cache_keys.reshape(2 * NKV * SEQC, DH), step_cache_values.reshape(NKV, SEQC, DV),
        w_out.reshape(DV, D), out_gain.reshape(1, DV), prompt_len, step_lens, mix_ratio,
    )
    return (
        piece_out, step_out,
        k[:ROWS].reshape(ROWS, 1, 2, DH), piece_v.reshape(ROWS, 1, DV),
        k[ROWS : ROWS + 1].reshape(1, 1, 2, DH), step_v.reshape(1, 1, DV),
    )


def solution(mesh):
    in_specs = (
        P("kv", None),
        P("kv", None),
        P(),
        P(None, "tp", None, None),
        P(None, "tp", None, None),
        P(None, "tp", None),
        P("tp", None, None),
        P("tp"),
        P(),
        P("kv", "tp", None, None),
        P("kv", "tp", None),
        P(None, "kv", "tp", None, None),
        P(None, "kv", "tp", None),
        P(),
        P(),
    )
    out_specs = (
        P("kv", "tp"),
        P("kv", "tp"),
        P("kv", "tp", None, None),
        P("kv", "tp", None),
        P("kv", "tp", None, None),
        P("kv", "tp", None),
    )
    return jax.shard_map(
        on_device, mesh=mesh, in_specs=in_specs, out_specs=out_specs, check_vma=False
    )
```

time: 128 us -> 110 us (0.86); the launches traced: 128 us -> 108 us
  starting transfers between devices: 12.5 us -> 0 us
  waiting for transfers between devices: 10.5 us -> 0 us
  Pallas kernels: 82.7 us -> 92.1 us
  local copies, waits for them, and re-layouts: 11.1 us -> 6.7 us
  matrix products: 6.93 us -> 4.53 us
    all_to_all x1 -> x0, starting transfers between devices: 12.5 us -> none  [summed_on_arrival(): blocks = lax.all_to_all(blocks, axis, 0, 0, tiled=True)]
    all_to_all x1 -> x0, waiting for transfers between devices: 10.5 us -> none  [summed_on_arrival(): blocks = lax.all_to_all(blocks, axis, 0, 0, tiled=True)]
    pallas_call x1, Pallas kernels: 82.7 us -> 92.1 us  [attention(): pl.pallas_call(attend, out_shape=(jax.ShapeDtypeStruct((ROWS, OUTB), BF16...]
    reshape x5 -> x0, local copies, waits for them, and re-layouts: 6.84 us -> none  [the longest x1 4.45 us: on_device(): step_cache_keys.reshape(NKV, SEQC, 2 * DH)]
    unnamed x20 -> x14, local copies, waits for them, and re-layouts: 1.81 us -> 5.45 us
    dot_general x3 -> x2, matrix products: 5.66 us -> 4.53 us  [project(): return jnp.dot(normed, flat_weight, preferred_element_type=F32).astype(BF16)]
  transfers between devices with their start and end apart: 1 -> 0, of which waited for: 1 -> 0; matrix products, arithmetic and copies ran while one was open for 2% -> 0% of each run, Pallas kernels for 0% -> 0%
where the time goes in v2:
time: 110 us; the launch traced here: 108 us
  Pallas kernels  92.1 us (84%)
  local copies, waits for them, and re-layouts  6.7 us (6%)
  matrix products  4.53 us (4%)
  other arithmetic  2.82 us (3%)
  between operations  2.02 us (2%)
    pallas_call x1, Pallas kernels, attention(): pl.pallas_call(attend, out_shape=(jax.ShapeDtypeStruct((ROWS, OUTB), BF16...  92.1 us
    unnamed x14, local copies, waits for them, and re-layouts  5.45 us
    dot_general x2, matrix products, project(): return jnp.dot(normed, flat_weight, preferred_element_type=F32).astype(BF16)  4.53 us

profile of v2, /device:TPU:1, one launch (start us, length us, event | category | flops | bytes accessed | tf_op | source)
XLA Modules:
  0.0 108.2 jit_solution(17358901391553525316)
XLA Ops:
  0.6 0.1 pad.2.clone
  0.7 1.5 %fusion.6 = f32[112]{0:T(128)S(1)} fusion(bf16[1,4096]{1,0:T(2,128)(2,1)} %param.16, bf16[96,4096]{1,0:T(8,128)(2,1)} %param.15, bf16[112]{0:T(256)(128)(2,1)S(1)} %pad.2.clone), kind=kLoop, calls=%fused_computation.8 | loop fusion | flops 3669904 | bytes 795296 | tf_op jit(solution)/shard_map/reduce_sum | solution.py:614
  2.3 0.0 copy-start
  2.3 0.0 copy-start.2
  2.3 0.0 copy-start.3
  2.3 0.0 copy-start.4
  2.3 3.3 %fusion.12.k_own = bf16[112,256]{1,0:T(8,128)(2,1)} fusion(bf16[512,8,2,128]{3,2,1,0:T(2,128)(2,1)} %bitcast.35, f32[4096]{0:T(1024)} %param.17, f32[112]{0:T(128)S(1)} %add_rsqrt_fusion, bf16[1,4096]{1,0:T(2,128)(2,1)} %param.16, bf16[96,4096]{1,0:T(8,128)(2,1)} %param.15, bf16[112]{0:T(256)(128)(2,1)S(1)} %pad.2.clone), kind=kOutput, calls=%fused_computation.12 | convolution fusion | flops 239038464 | bytes 2966176 | tf_op jit(solution)/shard_map/dot_general | solution.py:620
  5.6 0.0 copy-done
  5.6 0.0 copy-done.2
  5.6 0.0 copy-done.3
  5.6 1.3 %fusion.8.normed = bf16[112,4096]{1,0:T(8,128)(2,1)} fusion(f32[4096]{0:T(1024)S(1)} %copy-done.3, f32[112]{0:T(128)S(1)} %add_rsqrt_fusion, bf16[1,4096]{1,0:T(2,128)(2,1)S(1)} %copy-done.2, bf16[96,4096]{1,0:T(8,128)(2,1)S(1)} %copy-done, bf16[112]{0:T(256)(128)(2,1)S(1)} %pad.2.clone), kind=kLoop, calls=%fused_computation.10 | loop fusion | flops 4128768 | bytes 1729184 | tf_op jit(solution)/shard_map/convert_element_type | solution.py:615
  6.9 0.0 copy-done.4
  6.9 1.3 %fusion.9.q_own = bf16[112,256]{1,0:T(8,128)(2,1)} fusion(bf16[512,8,2,128]{3,2,1,0:T(2,128)(2,1)S(1)} %bitcast.36, f32[4096]{0:T(1024)S(1)} %copy-done.3, f32[112]{0:T(128)S(1)} %add_rsqrt_fusion, bf16[1,4096]{1,0:T(2,128)(2,1)S(1)} %copy-done.2, bf16[96,4096]{1,0:T(8,128)(2,1)S(1)} %copy-done, bf16[112]{0:T(256)(128)(2,1)S(1)} %pad.2.clone), kind=kOutput, calls=%fused_computation.11 | convolution fusion | flops 239038464 | bytes 2966176 | tf_op jit(solution)/shard_map/dot_general | solution.py:620
  9.4 0.0 slice-start
  9.5 0.0 copy-start.1
  9.5 92.1 %attend.1 = (bf16[96,512]{1,0:T(8,128)(2,1)}, bf16[1,512]{1,0:T(2,128)(2,1)}, bf16[96,256]{1,0:T(8,128)(2,1)}, bf16[1,256]{1,0:T(2,128)(2,1)}) custom-call(bf16[112,256]{1,0:T(8,128)(2,1)} %fusion.9.q_own, bf16[112,256]{1,0:T(8,128)(2,1)} %fusion.12.k_own, bf16[112,4096]{1,0:T(8,128)(2,1)} %fusion.8.normed, bf16[4096,256]{1,0:T(8,128)(2,1)} %bitcast.25, ...), custom_call_target="tpu_custom_call" | custom-call | tf_op jit(solution)/shard_map/attend/pallas_call | solution.py:544
  101.6 0.0 slice-done
  101.6 0.6 reshape.69
  102.2 0.0 copy-done.1
  102.2 0.5 slice_reduce_fusion
  102.8 1.5 %copy.42 = bf16[96,512]{1,0:T(8,128)(2,1)} copy(bf16[96,512]{1,0:T(8,128)(2,1)} %get-tuple-element.26) | data formatting | bytes 196608
  104.3 1.2 %copy.43 = bf16[1,512]{1,0:T(2,128)(2,1)} copy(bf16[1,512]{1,0:T(2,128)(2,1)} %get-tuple-element.27) | data formatting | bytes 2048
  105.5 1.4 %copy.44 = bf16[96,1,256]{2,0,1:T(8,128)(2,1)} copy(bf16[96,1,256]{2,0,1:T(8,128)(2,1)} %bitcast.32) | data formatting | bytes 98304
  107.0 1.2 %copy.45 = bf16[1,1,256]{2,1,0:T(2,128)(2,1)} copy(bf16[1,1,256]{2,1,0:T(2,128)(2,1)} %bitcast.34) | data formatting | bytes 1024
  (2 shorter events, 0.0 us)
Async XLA Ops:
  2.3 3.3 %copy-start = (bf16[96,4096]{1,0:T(8,128)(2,1)S(1)}, bf16[96,4096]{1,0:T(8,128)(2,1)}, u32[]{:S(2)}) copy-start(bf16[96,4096]{1,0:T(8,128)(2,1)} %param.15) | copy-start | bytes 2359300
  2.3 3.3 %copy-start.2 = (bf16[1,4096]{1,0:T(2,128)(2,1)S(1)}, bf16[1,4096]{1,0:T(2,128)(2,1)}, u32[]{:S(2)}) copy-start(bf16[1,4096]{1,0:T(2,128)(2,1)} %param.16) | copy-start | bytes 24580
  2.3 3.3 %copy-start.3 = (f32[4096]{0:T(1024)S(1)}, f32[4096]{0:T(1024)}, u32[]{:S(2)}) copy-start(f32[4096]{0:T(1024)} %param.17) | copy-start | bytes 49156
  2.3 4.6 %copy-start.4 = (bf16[4096,1,2,128]{3,2,1,0:T(2,128)(2,1)S(1)}, bf16[4096,1,2,128]{3,2,1,0:T(2,128)(2,1)}, u32[]{:S(2)}) copy-start(bf16[4096,1,2,128]{3,2,1,0:T(2,128)(2,1)} %param.18) | copy-start | bytes 6291460
  9.4 92.1 %slice-start = ((bf16[112,256]{1,0:T(8,128)(2,1)}), bf16[96,256]{1,0:T(8,128)(2,1)S(1)}, s32[]{:S(2)}) async-start(bf16[112,256]{1,0:T(8,128)(2,1)} %fusion.12.k_own), calls=%async_computation | async-start | bytes 98304 | tf_op jit(solution)/shard_map/slice | solution.py:639
  9.5 92.8 %copy-start.1 = (bf16[112,256]{1,0:T(8,128)(2,1)S(1)}, bf16[112,256]{1,0:T(8,128)(2,1)}, u32[]{:S(2)}) copy-start(bf16[112,256]{1,0:T(8,128)(2,1)} %fusion.12.k_own) | copy-start | bytes 172036

commit v3 on v2

--- a/solution.py
+++ b/solution.py
@@ -17,6 +17,7 @@
 R = ROWS // CHUNKS
 RD = 16
 TILE = NZ * R
+COUNT = CHUNKS * NY
 TILED = NZ * RD
 CACHE = 2048
 KEYS = CACHE + 128
@@ -30,9 +31,11 @@
 
 
 def attend(
-    q_own, k_own, normed, wv_hbm, kp_hbm, vp_hbm, kd_hbm, vd_hbm, wo_hbm, gain_ref, plen, slens, mix,
-    piece_ref, step_ref, pv_ref, sv_ref,
-    wv, wo, kraw, kfloat, kbuf, vnat, vt, kd, vdn, vtd, ksd, vse, qall, qd, bias, sbuf, pbuf, oacc,
+    tok_hbm, step_tok, in_gain, wq_hbm, wk_hbm, wv_hbm, kp_hbm, vp_hbm, kd_hbm, vd_hbm, wo_hbm,
+    gain_ref, plen, slens, mix,
+    out_ref,
+    tok, normed, wq, wk, wdeint, wv, wo, kraw, kfloat, kbuf, vnat, vt, kd, vdn, vtd, ksd, vse, qall, qd,
+    bias, sbuf, pbuf, mrow, oacc,
     stat, srecv, ressend, res, dsend, drecv, comb, rh, rf, acc, accb, rz, mixed,
     term, tsum, pr, th, tf,
     load_sem, zs, zr, ys, yr, hs, hr, ss, sr, rs, rr, xs, xr, fs, fr, ws, wr, ds, dr,
@@ -89,45 +92,66 @@
         )
 
     loads = [
-        pltpu.make_async_copy(wv_hbm, wv, load_sem.at[0]),
-        pltpu.make_async_copy(kp_hbm, kraw.at[pl.ds(0, 2 * CACHE), :], load_sem.at[1]),
-        pltpu.make_async_copy(vp_hbm, vnat, load_sem.at[2]),
-        pltpu.make_async_copy(kd_hbm, kraw.at[pl.ds(2 * CACHE, 2 * NKV * SEQC), :], load_sem.at[3]),
-        pltpu.make_async_copy(vd_hbm, vdn, load_sem.at[4]),
-        pltpu.make_async_copy(wo_hbm, wo, load_sem.at[5]),
+        pltpu.make_async_copy(tok_hbm, tok, load_sem.at[0]),
+        pltpu.make_async_copy(wq_hbm, wq, load_sem.at[1]),
+        pltpu.make_async_copy(wk_hbm, wk, load_sem.at[2]),
+        pltpu.make_async_copy(wv_hbm, wv, load_sem.at[3]),
+        pltpu.make_async_copy(kp_hbm, kraw.at[pl.ds(0, 2 * CACHE), :], load_sem.at[4]),
+        pltpu.make_async_copy(vp_hbm, vnat, load_sem.at[5]),
+        pltpu.make_async_copy(kd_hbm, kraw.at[pl.ds(2 * CACHE, 2 * NKV * SEQC), :], load_sem.at[6]),
+        pltpu.make_async_copy(vd_hbm, vdn, load_sem.at[7]),
+        pltpu.make_async_copy(wo_hbm, wo, load_sem.at[8]),
     ]
     for load in loads:
         load.start()
 
+    def norm(rows):
+        floats = rows.astype(F32)
+        inv_rms = lax.rsqrt(jnp.mean(floats * floats, axis=-1, keepdims=True) + EPS)
+        return (floats * inv_rms * in_gain[...]).astype(BF16)
+
+    last = norm(step_tok[...])
+    normed[ROWS:, :] = jnp.concatenate([last, jnp.zeros((RD - 1, D), BF16)], axis=0)
+    loads[0].wait()
+
+    @pl.loop(0, ROWS // 16)
+    def _(b):
+        rows = pl.ds(pl.multiple_of(b * 16, 16), 16)
+        normed[rows, :] = norm(tok[rows, :])
+
+    def split_maps(src, src_block, put):
+        kfloat[...] = src[pl.ds(pl.multiple_of(src_block * 512, 512), 512), :].astype(F32)
+        for c in range(2):
+            put(c, kfloat[pl.ds(c, 256, 2), :].astype(BF16))
+
+    def projected(weights):
+        @pl.loop(0, D // 256)
+        def _(b):
+            def put(c, flat):
+                rows = pl.ds(pl.multiple_of(b * 256, 256), 256)
+                wdeint[rows, c * DH : (c + 1) * DH] = flat
+
+            split_maps(weights, b, put)
+
+        return jnp.dot(normed[...], wdeint[...], preferred_element_type=F32).astype(BF16)
+
+    loads[1].wait()
+    queries = projected(wq)
     for j in range(4):
         n = rows_of(j)
         lo = j * R if j < CHUNKS else ROWS
         mine = qtile(j, y)
-        mine[pl.ds(pl.multiple_of(z * n, n), n), :] = q_own[lo : lo + n, :]
-
-    pl.semaphore_wait(barrier, NKV - 1 + 3)
-
-    def z_copy(j, d):
-        n = rows_of(j)
-        zt = (z + d) % NZ
-        block = zblock(qtile(j, y), z, n)
-        return rcopy(block, block, zs.at[j], zr.at[j], zt * NY + y)
-
-    def z_all(j):
-        some = qtile(j, y).at[pl.ds(0, (NZ - 1) * rows_of(j)), :]
-        return rcopy(some, some, zs.at[j], zr.at[j], z * NY + yp)
-
-    for j in range(4):
-        for d in (1, 7, 2, 6, 3, 5, 4):
-            z_copy(j, d).start()
-
-    loads[0].wait()
+        mine[pl.ds(pl.multiple_of(z * n, n), n), :] = queries[lo : lo + n, :]
+    loads[2].wait()
+    keys = projected(wk)
+    out_ref[:, OUTB + DV :] = keys
+    loads[3].wait()
     values = jnp.dot(normed[...], wv[...], preferred_element_type=F32).astype(BF16)
-    pv_ref[...] = values[:ROWS, :]
-    sv_ref[...] = values[ROWS : ROWS + 1, :]
-    kbuf[CACHE : CACHE + ROWS, :] = k_own[:ROWS, :]
+    out_ref[:, OUTB : OUTB + DV] = values
+
+    kbuf[CACHE : CACHE + ROWS, :] = keys[:ROWS, :]
     kbuf[CACHE + ROWS :, :] = jnp.zeros((KEYS - CACHE - ROWS, 2 * DH), BF16)
-    ksd[:RD, :] = k_own[ROWS:, :]
+    ksd[:RD, :] = keys[ROWS:, :]
     ksd[RD:, :] = jnp.zeros((SEQC - RD, 2 * DH), BF16)
     tail = jnp.concatenate([values[:ROWS, :], jnp.zeros((128 - ROWS, DV), BF16)], axis=0)
     vt[:, CACHE:] = tail.T
@@ -137,27 +161,43 @@
     place = me * CACHE + half + lax.broadcasted_iota(jnp.int32, (half, 128), 0)
     bias[...] = jnp.where(place < plen[0], 0.0, -jnp.inf).astype(F32)
     mixed[...] = jnp.zeros((PADDED, DV), F32)
-    loads[1].wait()
-    loads[2].wait()
+    loads[4].wait()
+    loads[5].wait()
 
     @pl.loop(0, CACHE // 256)
     def _(b):
-        kfloat[...] = kraw[pl.ds(pl.multiple_of(b * 512, 512), 512), :].astype(F32)
-        rows = pl.ds(pl.multiple_of(b * 256, 256), 256)
-        for c in range(2):
-            kbuf[rows, c * DH : (c + 1) * DH] = kfloat[pl.ds(c, 256, 2), :].astype(BF16)
+        def put(c, flat):
+            kbuf[pl.ds(pl.multiple_of(b * 256, 256), 256), c * DH : (c + 1) * DH] = flat
+
+        split_maps(kraw, b, put)
 
     for b in range(CACHE // 256):
         vt[:, b * 256 : (b + 1) * 256] = vnat[b * 256 : (b + 1) * 256, :].T
-    loads[3].wait()
+    pl.semaphore_wait(barrier, NKV - 1 + 3)
+
+    def z_copy(j, d):
+        n = rows_of(j)
+        zt = (z + d) % NZ
+        block = zblock(qtile(j, y), z, n)
+        return rcopy(block, block, zs.at[j], zr.at[j], zt * NY + y)
+
+    def z_all(j):
+        some = qtile(j, y).at[pl.ds(0, (NZ - 1) * rows_of(j)), :]
+        return rcopy(some, some, zs.at[j], zr.at[j], z * NY + yp)
+
+    for j in range(4):
+        for d in (1, 7, 2, 6, 3, 5, 4):
+            z_copy(j, d).start()
+
+    loads[6].wait()
 
     @pl.loop(0, NKV // 2)
     def _(b):
-        kfloat[...] = kraw[pl.ds(pl.multiple_of(2 * CACHE + b * 512, 512), 512), :].astype(F32)
-        for c in range(2):
-            flat = kfloat[pl.ds(c, 256, 2), :].astype(BF16)
-            for s in range(2):
-                kd[2 * b + s, :, c * DH : (c + 1) * DH] = flat[s * SEQC : (s + 1) * SEQC]
+        def put(c, flat):
+            for part in range(2):
+                kd[2 * b + part, :, c * DH : (c + 1) * DH] = flat[part * SEQC : (part + 1) * SEQC]
+
+        split_maps(kraw, 2 * CACHE // 512 + b, put)
 
     def z_wait_y_send(j):
         z_all(j).wait_recv()
@@ -341,14 +381,103 @@
             u_copy(j, side).wait_recv()
         own = term[core, x, span(j), :].astype(F32) + pr[x, span(j), :].astype(F32)
         total = (own + tf[0, span(j), :].astype(F32) + tf[1, span(j), :].astype(F32)).astype(BF16)
-        if j < CHUNKS:
-            piece_ref[span(j), :] = total
-        else:
-            step_ref[...] = total[:1]
+        out_ref[span(j), :OUTB] = total
 
     KB = [(b * 256, 256) for b in range(CACHE // 256)] + [(CACHE, 128)]
 
-    @pl.loop(0, CHUNKS * NY)
+    def tile_of(t):
+        i = t % NY
+        yy = (y + jnp.where(i == 2, 3, jnp.where(i == 3, 2, i))) % NY
+        return t // NY, yy, (t // NY) * NY + yy
+
+    def piece_step(t):
+        j, yy, ta = tile_of(jnp.minimum(t, COUNT - 1))
+        tb = jnp.where((t >= 1) & (t <= COUNT), tile_of(jnp.maximum(t - 1, 0))[2], COUNT)
+        tc = jnp.where(t >= 2, tile_of(jnp.maximum(t - 2, 0))[2], COUNT)
+        lane = lax.broadcasted_iota(jnp.int32, (128, TILE), 1)
+        row = lax.broadcasted_iota(jnp.int32, (128, TILE), 0)
+        row_place = ((lane // R) * NY + yy) * ROWS + R * j + lane % R
+        fresh_ok = (row < ROWS) & (me * ROWS + row <= row_place)
+        for c in range(2):
+            cols = slice(c * DH, (c + 1) * DH)
+            q = qall[ta, :, cols]
+            m = mrow[c, 0:1, :]
+            top = jnp.full((8, TILE), -jnp.inf, F32)
+            total = jnp.zeros((8, TILE), F32)
+            out = jnp.zeros((DV, TILE), F32)
+            for at, size in KB:
+                out = out + jnp.dot(
+                    vt[:, at : at + size], pbuf[c, at : at + size, :], preferred_element_type=F32
+                )
+                w = jnp.exp2((sbuf[c, at : at + size, :] - m) * EXPC)
+                total = total + jnp.sum(w.reshape(size // 8, 8, TILE), axis=0)
+                pbuf[c, at : at + size, :] = w.astype(BF16)
+                s = lax.dot_general(kbuf[at : at + size, cols], q, NT, preferred_element_type=F32)
+                if at == CACHE:
+                    s = jnp.where(fresh_ok, s, -jnp.inf)
+                elif at >= half:
+                    b = bias[at - half : at - half + size, :]
+                    s = s + jnp.concatenate([b, b], axis=1)
+                sbuf[c, at : at + size, :] = s
+                top = jnp.maximum(top, jnp.max(s.reshape(size // 8, 8, TILE), axis=0))
+            oacc[tc, c] = out
+            total = jnp.sum(total, axis=0, keepdims=True)
+            for hh in range(2):
+                stat[tb, 2 * c + hh : 2 * c + hh + 1, :] = m[:, hh * 128 : (hh + 1) * 128]
+                stat[tb, 4 + 2 * c + hh : 5 + 2 * c + hh, :] = total[:, hh * 128 : (hh + 1) * 128]
+            mrow[c, 0:1, :] = jnp.max(top, axis=0, keepdims=True)
+
+    def decode_step(t):
+        lane = lax.broadcasted_iota(jnp.int32, (SEQC, TILED), 1)
+        row = lax.broadcasted_iota(jnp.int32, (SEQC, TILED), 0)
+        jobs = []
+        for part in range(2):
+            yy = 2 * (t - COUNT - 2) + part
+            q2 = qd[yy]
+            own = (lane // RD == jnp.where(yy == y, z, NZ)) & (row == 0)
+            limit = jnp.zeros((SEQC, TILED), jnp.int32)
+            for zz in range(NZ):
+                vtd[part, :, zz * SEQC : (zz + 1) * SEQC] = vdn[zz * NY + yy].T
+                limit = jnp.where(lane // RD == zz, slens[zz * NY + yy], limit)
+            seen = me * SEQC + row < limit
+            for c in range(2):
+                cols = slice(c * DH, (c + 1) * DH)
+                q = q2[:, cols]
+                s = jnp.full((SEQC, TILED), -jnp.inf, F32)
+                for zz in range(NZ):
+                    one = lax.dot_general(kd[zz * NY + yy, :, cols], q, NT, preferred_element_type=F32)
+                    s = jnp.where((lane // RD == zz) & seen, one, s)
+                extra = lax.dot_general(ksd[:, cols], q, NT, preferred_element_type=F32)
+                jobs.append((part, yy, c, s, jnp.where(own, extra, -jnp.inf)))
+        ready = []
+        for part, yy, c, s, extra in jobs:
+            m = jnp.max(jnp.maximum(s, extra), axis=0, keepdims=True)
+            w = jnp.exp2((s - m) * EXPC)
+            we = jnp.exp2((extra - m) * EXPC)
+            total = jnp.sum(w + we, axis=0, keepdims=True)
+            for zz in range(NZ):
+                b = zz * NY + yy
+                dsend[b, 4 + c : 5 + c, :] = m
+                dsend[b, 6 + c : 7 + c, :] = total
+            ready.append((part, yy, c, w, we))
+        for part, yy, c, w, we in ready:
+            out = jnp.dot(vse[...], we.astype(BF16), preferred_element_type=F32)
+            for zz in range(NZ):
+                some = jnp.where(lane // RD == zz, w, 0.0).astype(BF16)
+                out = out + jnp.dot(
+                    vtd[part, :, zz * SEQC : (zz + 1) * SEQC], some, preferred_element_type=F32
+                )
+            out = out.T
+            for zz in range(NZ):
+                for hh in range(2):
+                    dsend[zz * NY + yy, 2 * c + hh : 2 * c + hh + 1, :] = out[
+                        RD * zz : RD * zz + 1, hh * 128 : (hh + 1) * 128
+                    ]
+
+    loads[7].wait()
+    loads[8].wait()
+
+    @pl.loop(0, COUNT + 4)
     def _(t):
         for step, work, arg in (
             (0, z_wait_y_send, 0),
@@ -357,97 +486,24 @@
             (2, z_wait_y_send, 2),
             (3, h_wait, 0),
             (3, z_wait_y_send, 3),
-            (4, stats_send, 0),
             (4, y_wait_fwd, 1),
-            (5, y_wait_fwd, 2),
-            (6, y_wait_fwd, 3),
+            (5, stats_send, 0),
+            (6, y_wait_fwd, 2),
             (7, h_wait, 1),
-            (7, stats_own, 0),
-            (8, stats_send, 1),
-            (10, rs_first, 0),
+            (8, y_wait_fwd, 3),
+            (9, stats_send, 1),
+            (9, stats_own, 0),
             (11, h_wait, 2),
-            (11, stats_own, 1),
-            (11, rs_second, 0),
+            (13, rs_first, 0),
+            (13, stats_own, 1),
+            (13, stats_send, 2),
+            (14, h_wait, 3),
+            (15, rs_second, 0),
+            (15, rs_first, 1),
         ):
             pl.when(t == step)(functools.partial(work, arg))
-
-        j = t // NY
-        i = t % NY
-        yy = (y + jnp.where(i == 2, 3, jnp.where(i == 3, 2, i))) % NY
-        tt = j * NY + yy
-        lane = lax.broadcasted_iota(jnp.int32, (128, TILE), 1)
-        row = lax.broadcasted_iota(jnp.int32, (128, TILE), 0)
-        row_place = ((lane // R) * NY + yy) * ROWS + R * j + lane % R
-        fresh_ok = (row < ROWS) & (me * ROWS + row <= row_place)
-        for c in range(2):
-            cols = slice(c * DH, (c + 1) * DH)
-            q = qall[tt, :, cols]
-            top = jnp.full((8, TILE), -jnp.inf, F32)
-            for at, size in KB:
-                s = lax.dot_general(kbuf[at : at + size, cols], q, NT, preferred_element_type=F32)
-                if at == CACHE:
-                    s = jnp.where(fresh_ok, s, -jnp.inf)
-                elif at >= half:
-                    b = bias[at - half : at - half + size, :]
-                    s = s + jnp.concatenate([b, b], axis=1)
-                sbuf[c, at : at + size, :] = s
-                top = jnp.maximum(top, jnp.max(s.reshape(size // 8, 8, TILE), axis=0))
-            m = jnp.max(top, axis=0, keepdims=True)
-            total = jnp.zeros((8, TILE), F32)
-            for at, size in KB:
-                w = jnp.exp2((sbuf[c, at : at + size, :] - m) * EXPC)
-                total = total + jnp.sum(w.reshape(size // 8, 8, TILE), axis=0)
-                pbuf[c, at : at + size, :] = w.astype(BF16)
-            total = jnp.sum(total, axis=0, keepdims=True)
-            oacc[tt, c] = jnp.dot(vt[...], pbuf[c], preferred_element_type=F32)
-            for hh in range(2):
-                stat[tt, 2 * c + hh : 2 * c + hh + 1, :] = m[:, hh * 128 : (hh + 1) * 128]
-                stat[tt, 4 + 2 * c + hh : 5 + 2 * c + hh, :] = total[:, hh * 128 : (hh + 1) * 128]
-
-    stats_send(2)
-
-    loads[4].wait()
-    h_wait(3)
-
-    @pl.loop(0, NY)
-    def _(yy):
-        q2 = qd[yy]
-        lane = lax.broadcasted_iota(jnp.int32, (SEQC, TILED), 1)
-        row = lax.broadcasted_iota(jnp.int32, (SEQC, TILED), 0)
-        own = (lane // RD == jnp.where(yy == y, z, NZ)) & (row == 0)
-        limit = jnp.zeros((SEQC, TILED), jnp.int32)
-        for zz in range(NZ):
-            vtd[:, zz * SEQC : (zz + 1) * SEQC] = vdn[zz * NY + yy].T
-            limit = jnp.where(lane // RD == zz, slens[zz * NY + yy], limit)
-        seen = me * SEQC + row < limit
-        for c in range(2):
-            cols = slice(c * DH, (c + 1) * DH)
-            q = q2[:, cols]
-            s = jnp.full((SEQC, TILED), -jnp.inf, F32)
-            for zz in range(NZ):
-                one = lax.dot_general(kd[zz * NY + yy, :, cols], q, NT, preferred_element_type=F32)
-                s = jnp.where((lane // RD == zz) & seen, one, s)
-            extra = lax.dot_general(ksd[:, cols], q, NT, preferred_element_type=F32)
-            extra = jnp.where(own, extra, -jnp.inf)
-            m = jnp.max(jnp.maximum(s, extra), axis=0, keepdims=True)
-            w = jnp.exp2((s - m) * EXPC)
-            we = jnp.exp2((extra - m) * EXPC)
-            total = jnp.sum(w + we, axis=0, keepdims=True)
-            out = jnp.dot(vse[...], we.astype(BF16), preferred_element_type=F32)
-            for zz in range(NZ):
-                part = jnp.where(lane // RD == zz, w, 0.0).astype(BF16)
-                out = out + jnp.dot(
-                    vtd[:, zz * SEQC : (zz + 1) * SEQC], part, preferred_element_type=F32
-                )
-            out = out.T
-            for zz in range(NZ):
-                b = zz * NY + yy
-                for hh in range(2):
-                    dsend[b, 2 * c + hh : 2 * c + hh + 1, :] = out[
-                        RD * zz : RD * zz + 1, hh * 128 : (hh + 1) * 128
-                    ]
-                dsend[b, 4 + c : 5 + c, :] = m
-                dsend[b, 6 + c : 7 + c, :] = total
+        pl.when(t < COUNT + 2)(functools.partial(piece_step, t))
+        pl.when(t >= COUNT + 2)(functools.partial(decode_step, t))
 
     def d_copy(target):
         return rcopy(dsend.at[target], drecv.at[me], ds.at[0], dr.at[0], target)
@@ -477,33 +533,31 @@
         for hh in range(2):
             mixed[ROWS : ROWS + 1, hh * 128 : (hh + 1) * 128] = parts[0][hh] - mix[0] * parts[1][hh]
 
+    stats_own(2)
     rs_third(0)
-    rs_first(1)
-    stats_own(2)
     rs_second(1)
+    rs_first(2)
+    rs_third(1)
     rs_last(0)
-    loads[5].wait()
     project_out(0)
-    rs_third(1)
-    rs_first(2)
+    rs_second(2)
+    decode_row()
+    project_out(3)
     tp_first(0)
+    rs_third(2)
     rs_last(1)
     project_out(1)
-    rs_second(2)
+    tp_first(3)
     tp_second(0)
-    decode_row()
-    project_out(3)
-    rs_third(2)
     tp_first(1)
+    tp_second(3)
     tp_last(0)
-    tp_first(3)
-    tp_second(1)
-    tp_second(3)
     rs_last(2)
     project_out(2)
-    tp_last(1)
+    tp_second(1)
     tp_last(3)
     tp_first(2)
+    tp_last(1)
     tp_second(2)
     tp_last(2)
 
@@ -534,7 +588,7 @@
     d_all().wait_send()
 
 
-def attention(q, k, normed, wv, kp, vp, kd, vd, wo, gain, prompt_len, step_lens, mix):
+def attention(tok, step_tok, in_gain, wq, wk, wv, kp, vp, kd, vd, wo, gain, prompt_len, step_lens, mix):
     vmem = pl.BlockSpec(memory_space=pltpu.VMEM)
     anyw = pl.BlockSpec(memory_space=pl.ANY)
     smem = pl.BlockSpec(memory_space=pltpu.SMEM)
@@ -543,15 +597,15 @@
     nt = CHUNKS * NY
     return pl.pallas_call(
         attend,
-        out_shape=(
-            jax.ShapeDtypeStruct((ROWS, OUTB), BF16),
-            jax.ShapeDtypeStruct((1, OUTB), BF16),
-            jax.ShapeDtypeStruct((ROWS, DV), BF16),
-            jax.ShapeDtypeStruct((1, DV), BF16),
-        ),
-        in_specs=[vmem, vmem, vmem] + [anyw] * 6 + [vmem, smem, smem, smem],
-        out_specs=(vmem,) * 4,
+        out_shape=jax.ShapeDtypeStruct((PADDED, OUTB + 2 * DV), BF16),
+        in_specs=[anyw, vmem, vmem] + [anyw] * 8 + [vmem, smem, smem, smem],
+        out_specs=vmem,
         scratch_shapes=[
+            V((ROWS, D), BF16),
+            V((PADDED, D), BF16),
+            V((2 * D, DH), BF16),
+            V((2 * D, DH), BF16),
+            V((D, 2 * DH), BF16),
             V((D, DV), BF16),
             V((DV, D), BF16),
             V((2 * CACHE + 2 * NKV * SEQC, DH), BF16),
@@ -561,7 +615,7 @@
             V((DV, KEYS), BF16),
             V((NKV, SEQC, 2 * DH), BF16),
             V((NKV, SEQC, DV), BF16),
-            V((DV, NZ * SEQC), BF16),
+            V((2, DV, NZ * SEQC), BF16),
             V((SEQC, 2 * DH), BF16),
             V((DV, SEQC), BF16),
             V((nt, TILE, 2 * DH), BF16),
@@ -569,8 +623,9 @@
             V((CACHE // 2, 128), F32),
             V((2, KEYS, TILE), F32),
             V((2, KEYS, TILE), BF16),
-            V((nt, 2, DV, TILE), F32),
-            V((nt, 8, 128), F32),
+            V((2, 8, TILE), F32),
+            V((nt + 1, 2, DV, TILE), F32),
+            V((nt + 1, 8, 128), F32),
             V((CHUNKS, NKV, 8, 128), F32),
             V((CHUNKS, 8, 128), F32),
             V((nt, 8, 128), F32),
@@ -588,7 +643,7 @@
             V((NX, PADDED, OUTB), BF16),
             V((2, PADDED, OUTB // 2), BF16),
             V((2, PADDED, OUTB), BF16),
-            dma((6,)),
+            dma((9,)),
             dma((4,)), dma((4,)),
             dma((4, 2)), dma((4, 2)),
             dma((4, 2)), dma((4, 2)),
@@ -606,38 +661,43 @@
             collective_id=0, has_side_effects=True, vmem_limit_bytes=62 << 20
         ),
         name="attend",
-    )(q, k, normed, wv, kp, vp, kd, vd, wo, gain, prompt_len, step_lens, mix)
-
-
-def norm_rows(tokens, in_gain):
-    floats = tokens.astype(F32)
-    inv_rms = lax.rsqrt(jnp.mean(floats * floats, axis=-1, keepdims=True) + EPS)
-    return (floats * inv_rms * in_gain).astype(BF16)
-
-
-def project(normed, weight):
-    flat_weight = weight.reshape(weight.shape[0], -1)
-    return jnp.dot(normed, flat_weight, preferred_element_type=F32).astype(BF16)
+    )(tok, step_tok, in_gain, wq, wk, wv, kp, vp, kd, vd, wo, gain, prompt_len, step_lens, mix)
+
+
+def split_outputs(all_ref, piece_ref, step_ref, pk_ref, pv_ref, sk_ref, sv_ref, flat):
+    piece_ref[...] = all_ref[:ROWS, :OUTB]
+    step_ref[...] = all_ref[ROWS : ROWS + 1, :OUTB]
+    pv_ref[...] = all_ref[:ROWS, OUTB : OUTB + DV]
+    sv_ref[...] = all_ref[ROWS : ROWS + 1, OUTB : OUTB + DV]
+    for c in range(2):
+        at = OUTB + DV + c * DH
+        flat[pl.ds(c, PADDED, 2), :] = all_ref[:, at : at + DH].astype(F32)
+    pk_ref[...] = flat[: 2 * ROWS, :].astype(BF16)
+    sk_ref[...] = flat[2 * ROWS : 2 * ROWS + 2, :].astype(BF16)
 
 
 def on_device(
     piece_tokens, step_tokens, in_gain, w_query, w_key, w_value, w_out, mix_ratio, out_gain,
     prompt_keys, prompt_values, step_cache_keys, step_cache_values, prompt_len, step_lens,
 ):
-    pad = jnp.zeros((RD - 1, piece_tokens.shape[1]), BF16)
-    normed = norm_rows(jnp.concatenate([piece_tokens, step_tokens, pad], axis=0), in_gain)
-    q = project(normed, w_query)
-    k = project(normed, w_key)
-    piece_out, step_out, piece_v, step_v = attention(
-        q, k, normed, w_value.reshape(D, DV),
+    together = attention(
+        piece_tokens, step_tokens, in_gain.reshape(1, D),
+        w_query.reshape(2 * D, DH), w_key.reshape(2 * D, DH), w_value.reshape(D, DV),
         prompt_keys.reshape(2 * CACHE, DH), prompt_values.reshape(CACHE, DV),
         step_cache_keys.reshape(2 * NKV * SEQC, DH), step_cache_values.reshape(NKV, SEQC, DV),
         w_out.reshape(DV, D), out_gain.reshape(1, DV), prompt_len, step_lens, mix_ratio,
     )
+    shapes = ((ROWS, OUTB), (1, OUTB), (2 * ROWS, DH), (ROWS, DV), (2, DH), (1, DV))
+    piece_out, step_out, piece_k, piece_v, step_k, step_v = pl.pallas_call(
+        split_outputs,
+        out_shape=tuple(jax.ShapeDtypeStruct(shape, BF16) for shape in shapes),
+        scratch_shapes=[pltpu.VMEM((2 * PADDED, DH), F32)],
+        name="split",
+    )(together)
     return (
         piece_out, step_out,
-        k[:ROWS].reshape(ROWS, 1, 2, DH), piece_v.reshape(ROWS, 1, DV),
-        k[ROWS : ROWS + 1].reshape(1, 1, 2, DH), step_v.reshape(1, 1, DV),
+        piece_k.reshape(ROWS, 1, 2, DH), piece_v.reshape(ROWS, 1, DV),
+        step_k.reshape(1, 1, 2, DH), step_v.reshape(1, 1, DV),
     )
 
 

time: 110 us -> 89.3 us (0.81)
  local copies, waits for them, and re-layouts: 6.7 us -> 0 us
  Pallas kernels: 92.1 us -> 86.2 us
  matrix products: 4.53 us -> 0 us
  other arithmetic: 2.82 us -> 0 us
    pallas_call x1 -> x2, Pallas kernels: 92.1 us -> 86.2 us  [the longest x1 84.5 us: attention(): pl.pallas_call(attend, out_shape=jax.ShapeDtypeStruct((PADDED, OUTB + 2 *...]
    unnamed x14 -> x0, local copies, waits for them, and re-layouts: 5.45 us -> none
    dot_general x2 -> x0, matrix products: 4.53 us -> none  [project(): return jnp.dot(normed, flat_weight, preferred_element_type=F32).astype(BF16)]
    reduce_sum x1 -> x0, other arithmetic: 1.54 us -> none  [norm_rows(): inv_rms = lax.rsqrt(jnp.mean(floats * floats, axis=-1, keepdims=True) + EPS)]
    convert_element_type x1 -> x0, other arithmetic: 1.27 us -> none  [norm_rows(): return (floats * inv_rms * in_gain).astype(BF16)]
where the time goes in v3:
time: 89.3 us; the launch traced here: 88.1 us
  Pallas kernels  86.2 us (97%)
  between operations  1.94 us (2%)
    pallas_call x1, Pallas kernels, attention(): pl.pallas_call(attend, out_shape=jax.ShapeDtypeStruct((PADDED, OUTB + 2 *...  84.5 us

profile of v3, /device:TPU:1, one launch (start us, length us, event | category | flops | bytes accessed | tf_op | source)
XLA Modules:
  0.0 88.1 jit_solution(14383704293364403805)
XLA Ops:
  1.9 84.5 %attend.1.all_ref = bf16[112,1024]{1,0:T(8,128)(2,1)} custom-call(bf16[96,4096]{1,0:T(8,128)(2,1)} %tok_hbm.1, bf16[1,4096]{1,0:T(2,128)(2,1)} %step_tok.1, f32[1,4096]{1,0:T(1,128)} %bitcast.24, bf16[8192,128]{1,0:T(8,128)(2,1)} %bitcast.16, bf16[8192,128]{1,0:T(8,128)(2,1)} %bitcast.17, bf16[4096,256]{1,0:T(8,128)(2,1)} %bitcast.18, ...), custom_call_target="tpu_custom_call" | custom-call | tf_op jit(solution)/shard_map/attend/pallas_call | solution.py:598
  86.5 1.6 %split.1 = (bf16[96,512]{1,0:T(8,128)(2,1)}, bf16[1,512]{1,0:T(2,128)(2,1)}, bf16[192,128]{1,0:T(8,128)(2,1)}, bf16[96,256]{1,0:T(8,128)(2,1)}, bf16[2,128]{1,0:T(2,128)(2,1)}, /*index=5*/bf16[1,256]{1,0:T(2,128)(2,1)}) custom-call(bf16[112,1024]{1,0:T(8,128)(2,1)} %attend.1.all_ref), custom_call_target="tpu_custom_call" | custom-call | tf_op jit(solution)/shard_map/split/pallas_call | solution.py:691

commit v4 on v3

--- a/solution.py
+++ b/solution.py
@@ -26,6 +26,7 @@
 PADDED = ROWS + RD
 EXPC = DH ** (-0.5) * math.log2(math.e)
 STAT_Z = (1, 4, 7)
+BATCHES = ((0,), (1, 7), (2, 6), (3, 5, 4))
 F32, BF16 = jnp.float32, jnp.bfloat16
 NT = (((1,), (1,)), ((), ()))
 
@@ -37,9 +38,9 @@
     tok, normed, wq, wk, wdeint, wv, wo, kraw, kfloat, kbuf, vnat, vt, kd, vdn, vtd, ksd, vse, qall, qd,
     bias, sbuf, pbuf, mrow, oacc,
     stat, srecv, ressend, res, dsend, drecv, comb, rh, rf, acc, accb, rz, mixed,
-    term, tsum, pr, th, tf,
+    term, tsum, pr, tf,
     load_sem, zs, zr, ys, yr, hs, hr, ss, sr, rs, rr, xs, xr, fs, fr, ws, wr, ds, dr,
-    ps, ps_r, ts, tr, us, ur,
+    ps, ps_r, us, ur,
 ):
     me = lax.axis_index("kv")
     tp = lax.axis_index("tp")
@@ -76,20 +77,6 @@
 
     def zblock(view, zz, n):
         return view.at[pl.ds(pl.multiple_of(zz * n, n), n), :]
-
-    barrier = pltpu.get_barrier_semaphore()
-
-    @pl.loop(1, NKV)
-    def _(d):
-        pl.semaphore_signal(
-            barrier, inc=1, device_id=at_kv((me + d) % NKV),
-            device_id_type=pl.DeviceIdType.MESH,
-        )
-
-    for tx, tc in ((x, 1 - core), (xp, core), (xm, core)):
-        pl.semaphore_signal(
-            barrier, inc=1, device_id={"tp": tx * 2 + tc}, device_id_type=pl.DeviceIdType.MESH
-        )
 
     loads = [
         pltpu.make_async_copy(tok_hbm, tok, load_sem.at[0]),
@@ -102,8 +89,22 @@
         pltpu.make_async_copy(vd_hbm, vdn, load_sem.at[7]),
         pltpu.make_async_copy(wo_hbm, wo, load_sem.at[8]),
     ]
-    for load in loads:
+    for load in loads[:2]:
         load.start()
+
+    barrier = pltpu.get_barrier_semaphore()
+
+    @pl.loop(1, NKV)
+    def _(d):
+        pl.semaphore_signal(
+            barrier, inc=1, device_id=at_kv((me + d) % NKV),
+            device_id_type=pl.DeviceIdType.MESH,
+        )
+
+    for tx, tc in ((x, 1 - core), (xp, core), (x2, core), (xm, core)):
+        pl.semaphore_signal(
+            barrier, inc=1, device_id={"tp": tx * 2 + tc}, device_id_type=pl.DeviceIdType.MESH
+        )
 
     def norm(rows):
         floats = rows.astype(F32)
@@ -113,6 +114,8 @@
     last = norm(step_tok[...])
     normed[ROWS:, :] = jnp.concatenate([last, jnp.zeros((RD - 1, D), BF16)], axis=0)
     loads[0].wait()
+    for load in loads[2:]:
+        load.start()
 
     @pl.loop(0, ROWS // 16)
     def _(b):
@@ -142,6 +145,52 @@
         lo = j * R if j < CHUNKS else ROWS
         mine = qtile(j, y)
         mine[pl.ds(pl.multiple_of(z * n, n), n), :] = queries[lo : lo + n, :]
+
+    def batch_sem(d):
+        return {0: 0, 1: 1, 7: 1, 2: 2, 6: 2}.get(d, 3)
+
+    def origin(d):
+        return (z + NZ - d) % NZ
+
+    def z_copy(j, d):
+        block = zblock(qtile(j, y), z, rows_of(j))
+        sem = zr.at[j, batch_sem(d)] if j < CHUNKS else zr.at[j, 0]
+        return rcopy(block, block, zs.at[j], sem, ((z + d) % NZ) * NY + y)
+
+    def z_some(j, count, sem):
+        some = qtile(j, y).at[pl.ds(0, count * rows_of(j)), :]
+        return rcopy(some, some, zs.at[j], sem, z * NY + yp)
+
+    def z_all(j):
+        return z_some(j, NZ - 1, zr.at[j, 0])
+
+    def z_send(j):
+        for d in (4, 3, 5, 2, 6, 1, 7):
+            z_copy(j, d).start()
+
+    def side_kv(side):
+        return z * NY + (yp if side == 0 else ym)
+
+    def z_relay(j, k):
+        if k > 0:
+            z_some(j, len(BATCHES[k]), zr.at[j, k]).wait_recv()
+        for d in BATCHES[k]:
+            block = zblock(qtile(j, y), origin(d), R)
+            for side in (0, 1):
+                rcopy(block, block, ys.at[j, side], yr.at[j, k], side_kv(side)).start()
+
+    def y_relay(j, k):
+        z_some(j, 2 * len(BATCHES[k]), yr.at[j, k]).wait_recv()
+        for side in (0, 1):
+            for d in BATCHES[k]:
+                if (side == 0) == (d < NZ // 2):
+                    block = zblock(qtile(j, ym if side == 0 else yp), origin(d), R)
+                    rcopy(block, block, hs.at[j, side], hr.at[j, 0], side_kv(side)).start()
+
+    pl.semaphore_wait(barrier, NKV - 1 + 4)
+    z_send(0)
+    z_relay(0, 0)
+
     loads[2].wait()
     keys = projected(wk)
     out_ref[:, OUTB + DV :] = keys
@@ -173,22 +222,6 @@
 
     for b in range(CACHE // 256):
         vt[:, b * 256 : (b + 1) * 256] = vnat[b * 256 : (b + 1) * 256, :].T
-    pl.semaphore_wait(barrier, NKV - 1 + 3)
-
-    def z_copy(j, d):
-        n = rows_of(j)
-        zt = (z + d) % NZ
-        block = zblock(qtile(j, y), z, n)
-        return rcopy(block, block, zs.at[j], zr.at[j], zt * NY + y)
-
-    def z_all(j):
-        some = qtile(j, y).at[pl.ds(0, (NZ - 1) * rows_of(j)), :]
-        return rcopy(some, some, zs.at[j], zr.at[j], z * NY + yp)
-
-    for j in range(4):
-        for d in (1, 7, 2, 6, 3, 5, 4):
-            z_copy(j, d).start()
-
     loads[6].wait()
 
     @pl.loop(0, NKV // 2)
@@ -206,7 +239,8 @@
 
     def y_copy(j, side):
         tile = qtile(j, y)
-        return rcopy(tile, tile, ys.at[j, side], yr.at[j, side], z * NY + (yp if side == 0 else ym))
+        sem = yr.at[j, side]
+        return rcopy(tile, tile, ys.at[j, side], sem, side_kv(side))
 
     def half_of(view, j, side):
         h = NZ * rows_of(j) // 2
@@ -214,7 +248,7 @@
 
     def h_copy(j, side):
         part = half_of(qtile(j, ym if side == 0 else yp), j, side)
-        return rcopy(part, part, hs.at[j, side], hr.at[j, side], z * NY + (yp if side == 0 else ym))
+        return rcopy(part, part, hs.at[j, side], hr.at[j, side], side_kv(side))
 
     def y_wait_fwd(j):
         for side in (0, 1):
@@ -223,6 +257,10 @@
             h_copy(j, side).start()
 
     def h_wait(j):
+        if j < CHUNKS:
+            tile = qtile(j, y2)
+            rcopy(tile, tile, hs.at[j, 0], hr.at[j, 0], z * NY + yp).wait_recv()
+            return
         for side in (0, 1):
             part = half_of(qtile(j, y2), j, side)
             rcopy(part, part, hs.at[j, side], hr.at[j, side], z * NY + yp).wait_recv()
@@ -348,40 +386,28 @@
                 term[tc, tx, span(j), :] = one.astype(BF16)
         p_copy(j).start()
 
-    def t_copy(j, side):
-        cols = slice(side * OUTB // 2, (side + 1) * OUTB // 2)
-        return tcopy(
-            tsum.at[x2, span(j), cols], th.at[side, span(j), :], ts.at[j, side], tr.at[j, side],
-            xp if side == 0 else xm, core,
-        )
-
-    def u_copy(j, side):
-        to = xp if side == 0 else xm
-        return tcopy(tsum.at[to, span(j), :], tf.at[side, span(j), :], us.at[j, side], ur.at[j, side], to, core)
+    def u_copy(j, d):
+        to = (x + d) % NX
+        return tcopy(tsum.at[to, span(j), :], tf.at[d - 1, span(j), :], us.at[j], ur.at[j], to, core)
+
+    def u_all(j):
+        some = tf.at[:, span(j), :]
+        return tcopy(some, some, us.at[j], ur.at[j], xp, core)
 
     def tp_first(j):
         p_copy(j).wait_recv()
         for tx in range(NX):
             both = term[core, tx, span(j), :].astype(F32) + pr[tx, span(j), :].astype(F32)
             tsum[tx, span(j), :] = both.astype(BF16)
-        for side in (0, 1):
-            t_copy(j, side).start()
-
-    def tp_second(j):
-        for side in (0, 1):
-            t_copy(j, side).wait_recv()
-            to = xp if side == 0 else xm
-            cols = slice(side * OUTB // 2, (side + 1) * OUTB // 2)
-            both = tsum[to, span(j), cols].astype(F32) + th[side, span(j), :].astype(F32)
-            tsum[to, span(j), cols] = both.astype(BF16)
-            u_copy(j, side).start()
+        for d in (2, 1, 3):
+            u_copy(j, d).start()
 
     def tp_last(j):
-        for side in (0, 1):
-            u_copy(j, side).wait_recv()
-        own = term[core, x, span(j), :].astype(F32) + pr[x, span(j), :].astype(F32)
-        total = (own + tf[0, span(j), :].astype(F32) + tf[1, span(j), :].astype(F32)).astype(BF16)
-        out_ref[span(j), :OUTB] = total
+        u_all(j).wait_recv()
+        total = term[core, x, span(j), :].astype(F32) + pr[x, span(j), :].astype(F32)
+        for d in range(NX - 1):
+            total = total + tf[d, span(j), :].astype(F32)
+        out_ref[span(j), :OUTB] = total.astype(BF16)
 
     KB = [(b * 256, 256) for b in range(CACHE // 256)] + [(CACHE, 128)]
 
@@ -477,31 +503,35 @@
     loads[7].wait()
     loads[8].wait()
 
+    events = (
+        ((z_relay, 0, 1), (z_relay, 0, 2), (z_relay, 0, 3), (z_send, 1)),
+        ((y_relay, 0, 0), (y_relay, 0, 1), (y_relay, 0, 2), (y_relay, 0, 3), (z_relay, 1, 0), (z_relay, 1, 1)),
+        ((z_relay, 1, 2), (z_relay, 1, 3), (z_send, 2)),
+        ((h_wait, 0), (y_relay, 1, 0), (y_relay, 1, 1)),
+        ((y_relay, 1, 2), (y_relay, 1, 3), (z_relay, 2, 0), (z_relay, 2, 1)),
+        ((stats_send, 0), (z_relay, 2, 2), (z_relay, 2, 3), (z_send, 3)),
+        (),
+        ((h_wait, 1), (y_relay, 2, 0), (y_relay, 2, 1)),
+        ((stats_own, 0), (y_relay, 2, 2), (y_relay, 2, 3), (z_wait_y_send, 3)),
+        ((stats_send, 1),),
+        ((y_wait_fwd, 3),),
+        ((h_wait, 2),),
+        ((rs_first, 0), (stats_own, 1)),
+        ((stats_send, 2),),
+        ((h_wait, 3), (rs_second, 0)),
+        (),
+    )
+
     @pl.loop(0, COUNT + 4)
     def _(t):
-        for step, work, arg in (
-            (0, z_wait_y_send, 0),
-            (1, z_wait_y_send, 1),
-            (1, y_wait_fwd, 0),
-            (2, z_wait_y_send, 2),
-            (3, h_wait, 0),
-            (3, z_wait_y_send, 3),
-            (4, y_wait_fwd, 1),
-            (5, stats_send, 0),
-            (6, y_wait_fwd, 2),
-            (7, h_wait, 1),
-            (8, y_wait_fwd, 3),
-            (9, stats_send, 1),
-            (9, stats_own, 0),
-            (11, h_wait, 2),
-            (13, rs_first, 0),
-            (13, stats_own, 1),
-            (13, stats_send, 2),
-            (14, h_wait, 3),
-            (15, rs_second, 0),
-            (15, rs_first, 1),
-        ):
-            pl.when(t == step)(functools.partial(work, arg))
+        for step, jobs in enumerate(events):
+            if jobs:
+
+                def run(jobs=jobs):
+                    for work, *args in jobs:
+                        work(*args)
+
+                pl.when(t == step)(run)
         pl.when(t < COUNT + 2)(functools.partial(piece_step, t))
         pl.when(t >= COUNT + 2)(functools.partial(decode_step, t))
 
@@ -534,41 +564,38 @@
             mixed[ROWS : ROWS + 1, hh * 128 : (hh + 1) * 128] = parts[0][hh] - mix[0] * parts[1][hh]
 
     stats_own(2)
+    rs_first(1)
     rs_third(0)
     rs_second(1)
     rs_first(2)
-    rs_third(1)
     rs_last(0)
     project_out(0)
     rs_second(2)
+    rs_third(1)
+    tp_first(0)
     decode_row()
     project_out(3)
-    tp_first(0)
     rs_third(2)
     rs_last(1)
     project_out(1)
     tp_first(3)
-    tp_second(0)
     tp_first(1)
-    tp_second(3)
-    tp_last(0)
     rs_last(2)
     project_out(2)
-    tp_second(1)
+    tp_last(0)
     tp_last(3)
     tp_first(2)
     tp_last(1)
-    tp_second(2)
     tp_last(2)
 
     for j in range(4):
         z_all(j).wait_send()
         p_copy(j).wait_send()
+        u_all(j).wait_send()
         for side in (0, 1):
             y_copy(j, side).wait_send()
-            h_copy(j, side).wait_send()
-            t_copy(j, side).wait_send()
-            u_copy(j, side).wait_send()
+            half = half_of(qtile(j, y), j, side)
+            rcopy(half, half, hs.at[j, side], hr.at[j, side], z * NY + yp).wait_send()
     for j in range(CHUNKS):
         w_all(j).wait_send()
         for side in (0, 1):
@@ -641,11 +668,10 @@
             V((2, NX, PADDED, OUTB), BF16),
             V((NX, PADDED, OUTB), BF16),
             V((NX, PADDED, OUTB), BF16),
-            V((2, PADDED, OUTB // 2), BF16),
-            V((2, PADDED, OUTB), BF16),
+            V((NX - 1, PADDED, OUTB), BF16),
             dma((9,)),
-            dma((4,)), dma((4,)),
-            dma((4, 2)), dma((4, 2)),
+            dma((4,)), dma((4, 4)),
+            dma((4, 2)), dma((4, 4)),
             dma((4, 2)), dma((4, 2)),
             dma((3, NY)), dma((3,)),
             dma((3,)), dma((3, NY)),
@@ -654,8 +680,7 @@
             dma((3,)), dma((3,)),
             dma((1,)), dma((1,)),
             dma((4,)), dma((4,)),
-            dma((4, 2)), dma((4, 2)),
-            dma((4, 2)), dma((4, 2)),
+            dma((4,)), dma((4,)),
         ],
         compiler_params=pltpu.CompilerParams(
             collective_id=0, has_side_effects=True, vmem_limit_bytes=62 << 20

time: 89.3 us -> 81.9 us (0.917); the launches traced: 88.1 us -> 81.7 us
  Pallas kernels: 86.2 us -> 79.7 us
    pallas_call x1, Pallas kernels: 84.5 us -> 78.1 us  [attention(): pl.pallas_call(attend, out_shape=jax.ShapeDtypeStruct((PADDED, OUTB + 2 *...]
where the time goes in v4:
time: 81.9 us; the launch traced here: 81.7 us
  Pallas kernels  79.7 us (97%)
  between operations  1.94 us (2%)
    pallas_call x1, Pallas kernels, attention(): pl.pallas_call(attend, out_shape=jax.ShapeDtypeStruct((PADDED, OUTB + 2 *...  78.1 us

profile of v4, /device:TPU:1, one launch (start us, length us, event | category | flops | bytes accessed | tf_op | source)
XLA Modules:
  0.0 81.7 jit_solution(9956387050219502978)
XLA Ops:
  1.9 78.1 %attend.1.all_ref = bf16[112,1024]{1,0:T(8,128)(2,1)} custom-call(bf16[96,4096]{1,0:T(8,128)(2,1)} %tok_hbm.1, bf16[1,4096]{1,0:T(2,128)(2,1)} %step_tok.1, f32[1,4096]{1,0:T(1,128)} %bitcast.24, bf16[8192,128]{1,0:T(8,128)(2,1)} %bitcast.16, bf16[8192,128]{1,0:T(8,128)(2,1)} %bitcast.17, bf16[4096,256]{1,0:T(8,128)(2,1)} %bitcast.18, ...), custom_call_target="tpu_custom_call" | custom-call | tf_op jit(solution)/shard_map/attend/pallas_call | solution.py:625
  80.0 1.6 %split.1 = (bf16[96,512]{1,0:T(8,128)(2,1)}, bf16[1,512]{1,0:T(2,128)(2,1)}, bf16[192,128]{1,0:T(8,128)(2,1)}, bf16[96,256]{1,0:T(8,128)(2,1)}, bf16[2,128]{1,0:T(2,128)(2,1)}, /*index=5*/bf16[1,256]{1,0:T(2,128)(2,1)}) custom-call(bf16[112,1024]{1,0:T(8,128)(2,1)} %attend.1.all_ref), custom_call_target="tpu_custom_call" | custom-call | tf_op jit(solution)/shard_map/split/pallas_call | solution.py:716

commit v5 on v4

--- a/solution.py
+++ b/solution.py
@@ -36,7 +36,7 @@
     gain_ref, plen, slens, mix,
     out_ref,
     tok, normed, wq, wk, wdeint, wv, wo, kraw, kfloat, kbuf, vnat, vt, kd, vdn, vtd, ksd, vse, qall, qd,
-    bias, sbuf, pbuf, mrow, oacc,
+    bias, sbuf, mrow, oacc,
     stat, srecv, ressend, res, dsend, drecv, comb, rh, rf, acc, accb, rz, mixed,
     term, tsum, pr, tf,
     load_sem, zs, zr, ys, yr, hs, hr, ss, sr, rs, rr, xs, xr, fs, fr, ws, wr, ds, dr,
@@ -177,7 +177,7 @@
         for d in BATCHES[k]:
             block = zblock(qtile(j, y), origin(d), R)
             for side in (0, 1):
-                rcopy(block, block, ys.at[j, side], yr.at[j, k], side_kv(side)).start()
+                rcopy(block, block, ys.at[j], yr.at[j, k], side_kv(side)).start()
 
     def y_relay(j, k):
         z_some(j, 2 * len(BATCHES[k]), yr.at[j, k]).wait_recv()
@@ -185,7 +185,7 @@
             for d in BATCHES[k]:
                 if (side == 0) == (d < NZ // 2):
                     block = zblock(qtile(j, ym if side == 0 else yp), origin(d), R)
-                    rcopy(block, block, hs.at[j, side], hr.at[j, 0], side_kv(side)).start()
+                    rcopy(block, block, hs.at[j], hr.at[j], side_kv(side)).start()
 
     pl.semaphore_wait(barrier, NKV - 1 + 4)
     z_send(0)
@@ -240,7 +240,7 @@
     def y_copy(j, side):
         tile = qtile(j, y)
         sem = yr.at[j, side]
-        return rcopy(tile, tile, ys.at[j, side], sem, side_kv(side))
+        return rcopy(tile, tile, ys.at[j], sem, side_kv(side))
 
     def half_of(view, j, side):
         h = NZ * rows_of(j) // 2
@@ -248,27 +248,33 @@
 
     def h_copy(j, side):
         part = half_of(qtile(j, ym if side == 0 else yp), j, side)
-        return rcopy(part, part, hs.at[j, side], hr.at[j, side], side_kv(side))
+        return rcopy(part, part, hs.at[j], hr.at[j], side_kv(side))
 
     def y_wait_fwd(j):
         for side in (0, 1):
             tile = qtile(j, ym if side == 0 else yp)
-            rcopy(tile, tile, ys.at[j, side], yr.at[j, side], z * NY + yp).wait_recv()
+            rcopy(tile, tile, ys.at[j], yr.at[j, side], z * NY + yp).wait_recv()
             h_copy(j, side).start()
 
+    def h_all(j):
+        tile = qtile(j, y2)
+        return rcopy(tile, tile, hs.at[j], hr.at[j], z * NY + yp)
+
     def h_wait(j):
-        if j < CHUNKS:
-            tile = qtile(j, y2)
-            rcopy(tile, tile, hs.at[j, 0], hr.at[j, 0], z * NY + yp).wait_recv()
-            return
-        for side in (0, 1):
-            part = half_of(qtile(j, y2), j, side)
-            rcopy(part, part, hs.at[j, side], hr.at[j, side], z * NY + yp).wait_recv()
+        h_all(j).wait_recv()
+
+    def y_all(j):
+        two = qall.at[pl.ds(0, 2)] if j < CHUNKS else qd.at[pl.ds(0, 2)]
+        return rcopy(two, two, ys.at[j], yr.at[j, 0], z * NY + yp)
 
     def s_copy(j, yt):
         return rcopy(
-            stat.at[j * NY + yt], srecv.at[j, me], ss.at[j, yt], sr.at[j], STAT_Z[j] * NY + yt
+            stat.at[j * NY + yt], srecv.at[j, me], ss.at[j], sr.at[j], STAT_Z[j] * NY + yt
         )
+
+    def s_some(j, count):
+        some = stat.at[pl.ds(0, count)]
+        return rcopy(some, some, ss.at[j], rr.at[j], z * NY + yp)
 
     def stats_send(j):
         for yt in range(NY):
@@ -283,7 +289,7 @@
                 srecv[j, me] = stat[j * NY + yt]
 
     def r_copy(j, target):
-        return rcopy(ressend.at[j], res.at[j * NY + y], rs.at[j], rr.at[j, y], target)
+        return rcopy(ressend.at[j], res.at[j * NY + y], rs.at[j], rr.at[j], target)
 
     def stats_own(j):
         @pl.when(z == STAT_Z[j])
@@ -302,39 +308,42 @@
                 r_copy(j, (me + d) % NKV).start()
 
     def stats_wait(j):
-        for yt in range(NY):
-            owner = STAT_Z[j] * NY + yt
-
-            @pl.when(owner != me)
-            def _():
-                rcopy(ressend.at[j], res.at[j * NY + yt], rs.at[j], rr.at[j, yt], owner).wait_recv()
-
-    def combine(j):
-        @pl.loop(0, NY)
-        def _(yy):
-            tt = j * NY + yy
-            factors = []
-            for c in range(2):
-                pick = lambda ref, lo: jnp.concatenate(
-                    [ref[tt, lo + 2 * c + hh : lo + 2 * c + hh + 1, :] for hh in range(2)], axis=1
-                )
-                factors.append(jnp.exp2((pick(stat, 0) - pick(res, 0)) * EXPC) * pick(res, 4))
-            both = oacc[tt, 0] * factors[0] - oacc[tt, 1] * (factors[1] * mix[0])
-            comb[tt] = both.T.astype(BF16)
+        @pl.when(z == STAT_Z[j])
+        def _():
+            s_some(j, NY - 1).wait_recv()
+
+        @pl.when(z != STAT_Z[j])
+        def _():
+            s_some(j, NY).wait_recv()
+
+    def combine(j, yy):
+        tt = j * NY + yy
+        factors = []
+        for c in range(2):
+            pick = lambda ref, lo: jnp.concatenate(
+                [ref[tt, lo + 2 * c + hh : lo + 2 * c + hh + 1, :] for hh in range(2)], axis=1
+            )
+            factors.append(jnp.exp2((pick(stat, 0) - pick(res, 0)) * EXPC) * pick(res, 4))
+        both = oacc[tt, 0] * factors[0] - oacc[tt, 1] * (factors[1] * mix[0])
+        comb[tt] = both.T.astype(BF16)
 
     def x_copy(j, side):
         part = half_of(ctile(j, y2), j, side)
-        return rcopy(part, rh.at[j, side], xs.at[j, side], xr.at[j, side], z * NY + (yp if side == 0 else ym))
+        return rcopy(part, rh.at[j, side], xs.at[j], xr.at[j, side], z * NY + (yp if side == 0 else ym))
 
     def f_copy(j, side):
         tile = ctile(j, yp if side == 0 else ym)
-        return rcopy(tile, rf.at[j, side], fs.at[j, side], fr.at[j, side], z * NY + (yp if side == 0 else ym))
+        return rcopy(tile, rf.at[j, side], fs.at[j], fr.at[j, side], z * NY + (yp if side == 0 else ym))
 
     def rs_first(j):
         stats_wait(j)
-        combine(j)
+        combine(j, y2)
         for side in (0, 1):
             x_copy(j, side).start()
+
+        @pl.loop(1, NY)
+        def _(i):
+            combine(j, (y2 + i) % NY)
 
     def rs_second(j):
         for side in (0, 1):
@@ -379,12 +388,13 @@
         total = mixed[span(j), :]
         inv_rms = lax.rsqrt(jnp.mean(total * total, axis=-1, keepdims=True) + EPS)
         head = (total * inv_rms * gain_ref[...] * OUT_SCALE).astype(BF16)
-        for tx in range(NX):
-            for tc in range(2):
-                at = (tx * 2 + tc) * OUTB
-                one = jnp.dot(head, wo[:, at : at + OUTB], preferred_element_type=F32)
+        for tc in (1 - core, core):
+            for tx in range(NX):
+                at = pl.multiple_of((tx * 2 + tc) * OUTB, OUTB)
+                one = jnp.dot(head, wo[:, pl.ds(at, OUTB)], preferred_element_type=F32)
                 term[tc, tx, span(j), :] = one.astype(BF16)
-        p_copy(j).start()
+            if tc is not core:
+                p_copy(j).start()
 
     def u_copy(j, d):
         to = (x + d) % NX
@@ -416,10 +426,9 @@
         yy = (y + jnp.where(i == 2, 3, jnp.where(i == 3, 2, i))) % NY
         return t // NY, yy, (t // NY) * NY + yy
 
-    def piece_step(t):
+    def piece_step(t, scores=True):
         j, yy, ta = tile_of(jnp.minimum(t, COUNT - 1))
-        tb = jnp.where((t >= 1) & (t <= COUNT), tile_of(jnp.maximum(t - 1, 0))[2], COUNT)
-        tc = jnp.where(t >= 2, tile_of(jnp.maximum(t - 2, 0))[2], COUNT)
+        tb = jnp.where(t >= 1, tile_of(jnp.maximum(t - 1, 0))[2], COUNT)
         lane = lax.broadcasted_iota(jnp.int32, (128, TILE), 1)
         row = lax.broadcasted_iota(jnp.int32, (128, TILE), 0)
         row_place = ((lane // R) * NY + yy) * ROWS + R * j + lane % R
@@ -432,12 +441,13 @@
             total = jnp.zeros((8, TILE), F32)
             out = jnp.zeros((DV, TILE), F32)
             for at, size in KB:
-                out = out + jnp.dot(
-                    vt[:, at : at + size], pbuf[c, at : at + size, :], preferred_element_type=F32
-                )
                 w = jnp.exp2((sbuf[c, at : at + size, :] - m) * EXPC)
                 total = total + jnp.sum(w.reshape(size // 8, 8, TILE), axis=0)
-                pbuf[c, at : at + size, :] = w.astype(BF16)
+                out = out + jnp.dot(
+                    vt[:, at : at + size], w.astype(BF16), preferred_element_type=F32
+                )
+                if not scores:
+                    continue
                 s = lax.dot_general(kbuf[at : at + size, cols], q, NT, preferred_element_type=F32)
                 if at == CACHE:
                     s = jnp.where(fresh_ok, s, -jnp.inf)
@@ -446,19 +456,20 @@
                     s = s + jnp.concatenate([b, b], axis=1)
                 sbuf[c, at : at + size, :] = s
                 top = jnp.maximum(top, jnp.max(s.reshape(size // 8, 8, TILE), axis=0))
-            oacc[tc, c] = out
+            oacc[tb, c] = out
             total = jnp.sum(total, axis=0, keepdims=True)
             for hh in range(2):
                 stat[tb, 2 * c + hh : 2 * c + hh + 1, :] = m[:, hh * 128 : (hh + 1) * 128]
                 stat[tb, 4 + 2 * c + hh : 5 + 2 * c + hh, :] = total[:, hh * 128 : (hh + 1) * 128]
-            mrow[c, 0:1, :] = jnp.max(top, axis=0, keepdims=True)
+            if scores:
+                mrow[c, 0:1, :] = jnp.max(top, axis=0, keepdims=True)
 
     def decode_step(t):
         lane = lax.broadcasted_iota(jnp.int32, (SEQC, TILED), 1)
         row = lax.broadcasted_iota(jnp.int32, (SEQC, TILED), 0)
         jobs = []
         for part in range(2):
-            yy = 2 * (t - COUNT - 2) + part
+            yy = 2 * (t - COUNT - 1) + part
             q2 = qd[yy]
             own = (lane // RD == jnp.where(yy == y, z, NZ)) & (row == 0)
             limit = jnp.zeros((SEQC, TILED), jnp.int32)
@@ -508,21 +519,20 @@
         ((y_relay, 0, 0), (y_relay, 0, 1), (y_relay, 0, 2), (y_relay, 0, 3), (z_relay, 1, 0), (z_relay, 1, 1)),
         ((z_relay, 1, 2), (z_relay, 1, 3), (z_send, 2)),
         ((h_wait, 0), (y_relay, 1, 0), (y_relay, 1, 1)),
-        ((y_relay, 1, 2), (y_relay, 1, 3), (z_relay, 2, 0), (z_relay, 2, 1)),
-        ((stats_send, 0), (z_relay, 2, 2), (z_relay, 2, 3), (z_send, 3)),
+        ((z_relay, 2, 0), (z_relay, 2, 1)),
+        ((stats_send, 0), (y_relay, 1, 2), (y_relay, 1, 3), (z_relay, 2, 2), (z_relay, 2, 3), (z_send, 3)),
         (),
         ((h_wait, 1), (y_relay, 2, 0), (y_relay, 2, 1)),
         ((stats_own, 0), (y_relay, 2, 2), (y_relay, 2, 3), (z_wait_y_send, 3)),
         ((stats_send, 1),),
-        ((y_wait_fwd, 3),),
-        ((h_wait, 2),),
+        (),
+        ((h_wait, 2), (y_wait_fwd, 3)),
         ((rs_first, 0), (stats_own, 1)),
-        ((stats_send, 2),),
-        ((h_wait, 3), (rs_second, 0)),
-        (),
+        ((stats_send, 2), (h_wait, 3)),
+        ((rs_second, 0),),
     )
 
-    @pl.loop(0, COUNT + 4)
+    @pl.loop(0, COUNT + 3)
     def _(t):
         for step, jobs in enumerate(events):
             if jobs:
@@ -532,8 +542,9 @@
                         work(*args)
 
                 pl.when(t == step)(run)
-        pl.when(t < COUNT + 2)(functools.partial(piece_step, t))
-        pl.when(t >= COUNT + 2)(functools.partial(decode_step, t))
+        pl.when(t < COUNT)(functools.partial(piece_step, t))
+        pl.when(t == COUNT)(functools.partial(piece_step, t, False))
+        pl.when(t >= COUNT + 1)(functools.partial(decode_step, t))
 
     def d_copy(target):
         return rcopy(dsend.at[target], drecv.at[me], ds.at[0], dr.at[0], target)
@@ -563,18 +574,18 @@
         for hh in range(2):
             mixed[ROWS : ROWS + 1, hh * 128 : (hh + 1) * 128] = parts[0][hh] - mix[0] * parts[1][hh]
 
+    rs_first(1)
     stats_own(2)
-    rs_first(1)
     rs_third(0)
+    rs_first(2)
     rs_second(1)
-    rs_first(2)
     rs_last(0)
     project_out(0)
     rs_second(2)
     rs_third(1)
-    tp_first(0)
     decode_row()
     project_out(3)
+    tp_first(0)
     rs_third(2)
     rs_last(1)
     project_out(1)
@@ -590,27 +601,24 @@
 
     for j in range(4):
         z_all(j).wait_send()
+        y_all(j).wait_send()
+        h_all(j).wait_send()
         p_copy(j).wait_send()
         u_all(j).wait_send()
-        for side in (0, 1):
-            y_copy(j, side).wait_send()
-            half = half_of(qtile(j, y), j, side)
-            rcopy(half, half, hs.at[j, side], hr.at[j, side], z * NY + yp).wait_send()
     for j in range(CHUNKS):
         w_all(j).wait_send()
-        for side in (0, 1):
-            x_copy(j, side).wait_send()
-            f_copy(j, side).wait_send()
-        for yt in range(NY):
-
-            @pl.when(STAT_Z[j] * NY + yt != me)
-            def _():
-                s_copy(j, yt).wait_send()
+        rcopy(rf.at[j], rf.at[j], fs.at[j], fr.at[j, 0], z * NY + yp).wait_send()
+        rcopy(rh.at[j], rh.at[j], xs.at[j], xr.at[j, 0], z * NY + yp).wait_send()
 
         @pl.when(z == STAT_Z[j])
         def _():
             most = srecv.at[j, pl.ds(0, NKV - 1)]
             rcopy(most, most, rs.at[j], sr.at[j], z * NY + yp).wait_send()
+            s_some(j, NY - 1).wait_send()
+
+        @pl.when(z != STAT_Z[j])
+        def _():
+            s_some(j, NY).wait_send()
 
     d_all().wait_send()
 
@@ -649,7 +657,6 @@
             V((NY, TILED, 2 * DH), BF16),
             V((CACHE // 2, 128), F32),
             V((2, KEYS, TILE), F32),
-            V((2, KEYS, TILE), BF16),
             V((2, 8, TILE), F32),
             V((nt + 1, 2, DV, TILE), F32),
             V((nt + 1, 8, 128), F32),
@@ -671,12 +678,12 @@
             V((NX - 1, PADDED, OUTB), BF16),
             dma((9,)),
             dma((4,)), dma((4, 4)),
-            dma((4, 2)), dma((4, 4)),
-            dma((4, 2)), dma((4, 2)),
-            dma((3, NY)), dma((3,)),
-            dma((3,)), dma((3, NY)),
-            dma((3, 2)), dma((3, 2)),
-            dma((3, 2)), dma((3, 2)),
+            dma((4,)), dma((4, 4)),
+            dma((4,)), dma((4,)),
+            dma((3,)), dma((3,)),
+            dma((3,)), dma((3,)),
+            dma((3,)), dma((3, 2)),
+            dma((3,)), dma((3, 2)),
             dma((3,)), dma((3,)),
             dma((1,)), dma((1,)),
             dma((4,)), dma((4,)),

time: 81.9 us -> 78.5 us (0.958)
  Pallas kernels: 79.7 us -> 76.3 us
    pallas_call x1, Pallas kernels: 78.1 us -> 74.7 us  [attention(): pl.pallas_call(attend, out_shape=jax.ShapeDtypeStruct((PADDED, OUTB + 2 *...]
where the time goes in v5:
time: 78.5 us; the launch traced here: 78.3 us
  Pallas kernels  76.3 us (97%)
  between operations  1.94 us (2%)
    pallas_call x1, Pallas kernels, attention(): pl.pallas_call(attend, out_shape=jax.ShapeDtypeStruct((PADDED, OUTB + 2 *...  74.7 us
    pallas_call x1, Pallas kernels, on_device(): pl.pallas_call(split_outputs, out_shape=tuple((jax.ShapeDtypeStruct(shape...  1.63 us

profile of v5, /device:TPU:1, one launch (start us, length us, event | category | flops | bytes accessed | tf_op | source)
XLA Modules:
  0.0 78.3 jit_solution(5055204777776213765)
XLA Ops:
  1.9 74.7 %attend.1.all_ref = bf16[112,1024]{1,0:T(8,128)(2,1)} custom-call(bf16[96,4096]{1,0:T(8,128)(2,1)} %tok_hbm.1, bf16[1,4096]{1,0:T(2,128)(2,1)} %step_tok.1, f32[1,4096]{1,0:T(1,128)} %bitcast.24, bf16[8192,128]{1,0:T(8,128)(2,1)} %bitcast.16, bf16[8192,128]{1,0:T(8,128)(2,1)} %bitcast.17, bf16[4096,256]{1,0:T(8,128)(2,1)} %bitcast.18, ...), custom_call_target="tpu_custom_call" | custom-call | tf_op jit(solution)/shard_map/attend/pallas_call | solution.py:633
  76.6 1.6 %split.1 = (bf16[96,512]{1,0:T(8,128)(2,1)}, bf16[1,512]{1,0:T(2,128)(2,1)}, bf16[192,128]{1,0:T(8,128)(2,1)}, bf16[96,256]{1,0:T(8,128)(2,1)}, bf16[2,128]{1,0:T(2,128)(2,1)}, /*index=5*/bf16[1,256]{1,0:T(2,128)(2,1)}) custom-call(bf16[112,1024]{1,0:T(8,128)(2,1)} %attend.1.all_ref), custom_call_target="tpu_custom_call" | custom-call | tf_op jit(solution)/shard_map/split/pallas_call | solution.py:723
